TPU v7x, 512 devices: a whole 4x4x16 slice. The times are simulated.
512 devices in a mesh: sp: 64 (over z, y), tp: 8 (over x, core).
Axes of the slice: x: 4, y: 4, z: 16, core: 2. Of those that a mesh axis runs over, the one named last changes fastest.
Arguments:
- inputs: bfloat16 [16384, 4096], P('sp', 'tp'), may hold values from -20 to 20
- norm_gain: float32 [3, 4096], replicated, may hold values from 0.1 to 1.9
- in_weight: bfloat16 [3, 4096, 1024], P(None, 'tp', 'sp'), may hold values from -0.09375 to 0.09375
- pool_scale: float32 [3, 1024], replicated, may hold values from 0.1 to 1.9
- out_weight: bfloat16 [3, 1024, 4096], P(None, 'sp', 'tp'), may hold values from -0.1875 to 0.1875
Outputs:
- final_state: bfloat16 [16384, 4096], P('sp', 'tp')
All inputs are finite; a program needn't handle non-finite values.
Results may differ from a plain program's by a relative error of at most 0.017.
Values may be sent and summed in bfloat16 or wider, within the bound.
A program may use at most 64 MiB of HBM per device.

v0:
```python
import jax
import jax.numpy as jnp
from jax import lax
from jax.sharding import PartitionSpec as P

D = 4096
P_SIZE = 1024
LAYERS = 3


epsilon = 1e-06
halo_rows = 16
group_count = 4


def turned_gather(arrays, axis, dims):
    turned = [jnp.moveaxis(a, dim, 0) for a, dim in zip(arrays, dims)]
    both = jnp.concatenate([t.reshape(len(t), -1) for t in turned], axis=1)
    filled, at, gathered = (lax.all_gather(both, axis, axis=0, tiled=True), 0, [])
    for t, dim in zip(turned, dims):
        section = filled[:, at : at + t[0].size].reshape(-1, *t.shape[1:])
        gathered.append(jnp.moveaxis(section, 0, dim))
        at += t[0].size
    return tuple(gathered)


def copy_for_each(shard, axis):
    copies = jnp.broadcast_to(shard, (lax.axis_size(axis), *shard.shape))
    return lax.all_to_all(copies, axis, split_axis=0, concat_axis=0, tiled=True)


def taken_together(shard, axis):
    return copy_for_each(shard, axis).sum(axis=0)


def split_up(shard, dim, length):
    before, after = (shard.shape[:dim], shard.shape[dim + 1 :])
    return jnp.moveaxis(shard.reshape(*before, length, -1, *after), dim, 0)


def summed_on_arrival(shard, axis, dim):
    parts = split_up(shard, dim, lax.axis_size(axis))
    arrived = lax.all_to_all(parts, axis, split_axis=0, concat_axis=0, tiled=True)
    return arrived.astype(jnp.float32).sum(axis=0)


def from_behind(value, axis, steps):
    count = lax.axis_size(axis)
    initial, last = (max(0, -steps), min(count, count - steps))
    return lax.ppermute(value, axis, [(source, source + steps) for source in range(initial, last)])


def laid_out(parts, dim):
    dims = list(parts.shape[1:])
    dims[dim] *= parts.shape[0]
    return jnp.moveaxis(parts, 0, dim).reshape(dims)


def collect(shard, axis, dim):
    parts = copy_for_each(shard, axis)
    return laid_out(parts, dim)


def window_means(extended, row_count, first_channel, first_pos, pool_total):
    width = extended.shape[1]
    channel = first_channel + lax.broadcasted_iota(jnp.int32, (1, width), 1)
    group_index = channel // (pool_total // group_count)
    window_len = jnp.left_shift(jnp.int32(2), group_index)
    running = jnp.zeros((row_count, width), jnp.float32)
    for offset in range(halo_rows):
        shifted = extended[halo_rows - offset : halo_rows - offset + row_count]
        running = running + jnp.where(offset < window_len, shifted, 0.0)
    position = first_pos + lax.broadcasted_iota(jnp.int32, (row_count, 1), 0)
    divisor = jnp.minimum(position + 1, window_len).astype(jnp.float32)
    return running / divisor - extended[halo_rows:]


def body(inputs, norm_gain, in_weight, pool_scale, out_weight):
    row_count, feature_part = inputs.shape
    channel_part = P_SIZE // lax.axis_size("tp")
    tp_index = lax.axis_index("tp")
    sp_index = lax.axis_index("sp")
    current = inputs
    in_all, out_all = turned_gather((in_weight, out_weight), "sp", (2, 1))
    for layer_index in range(LAYERS):
        gain_row = norm_gain[layer_index]
        widened = current.astype(jnp.float32)
        squares = taken_together(jnp.sum(widened * widened, axis=1), "tp")
        inv_rms = lax.rsqrt(squares / D + epsilon)[:, None]
        own_gain = lax.dynamic_slice_in_dim(gain_row, tp_index * feature_part, feature_part)
        normed = (widened * inv_rms * own_gain).astype(jnp.bfloat16)
        partials = jnp.dot(normed, in_all[layer_index], preferred_element_type=jnp.float32)
        pool_in = summed_on_arrival(partials.astype(jnp.bfloat16), "tp", 1).astype(jnp.bfloat16)
        edge_block = from_behind(pool_in[row_count - halo_rows :], "sp", 1)
        extended = jnp.concatenate([edge_block, pool_in], 0).astype(jnp.float32)
        means = window_means(
            extended, row_count, tp_index * channel_part, sp_index * row_count, P_SIZE
        )
        own_scale = lax.dynamic_slice_in_dim(
            pool_scale[layer_index], tp_index * channel_part, channel_part
        )
        mixed = (means * own_scale).astype(jnp.bfloat16)
        all_pooled = collect(mixed, "tp", 1)
        branch = jnp.dot(all_pooled, out_all[layer_index], preferred_element_type=jnp.float32)
        current = (current.astype(jnp.float32) + branch).astype(jnp.bfloat16)
    return current


def solution(mesh):
    placed = (P("sp", "tp"), P(), P(None, "tp", "sp"), P(), P(None, "sp", "tp"))
    return jax.shard_map(body, mesh=mesh, in_specs=placed, out_specs=P("sp", "tp"), check_vma=False)
```

profile of v0, /device:TPU:32, one launch (start us, length us, event | category | flops | bytes accessed | tf_op | source)
XLA Modules:
  0.0 325.0 jit_solution(5768938478417234308)
XLA Ops:
  6.5 0.8 copy.74
  7.3 0.8 copy.73
  8.1 0.6 pad_maximum_fusion
  8.8 1.1 fusion.8
  9.9 0.6 broadcast_in_dim.258
  10.5 4.3 %all-to-all-start = ((f32[8,1,256]{2,1,0:T(1,128)}), f32[8,1,256]{2,1,0:T(1,128)S(1)}, u32[]{:S(2)}, u32[]{:S(2)}) async-start(f32[8,1,256]{2,1,0:T(1,128)} %broadcast_in_dim.258), calls=%async_computation | async-start | bytes 16384 | tf_op jit(solution)/shard_map/all_to_all | solution.py:29
  15.5 1.6 fusion.80
  17.7 2.4 all-to-all-done
  20.2 145.4 %all-gather.2.cloned.1.call-done = bf16[1024,3072]{1,0:T(8,128)(2,1)} async-done(((bf16[16,3072]{1,0:T(8,128)(2,1)}), bf16[1024,3072]{1,0:T(8,128)(2,1)}) %all-gather.2.cloned.1.call-update) | async-done | bytes 6291472 | tf_op jit(solution)/shard_map/all_gather | solution.py:19
  165.6 5.0 %fusion.79 = (bf16[1024,1536]{1,0:T(8,128)(2,1)S(1)}, bf16[1024,1536]{1,0:T(8,128)(2,1)}) fusion(bf16[1024,3072]{1,0:T(8,128)(2,1)} %all-gather.2.cloned.1.call-done), kind=kLoop, calls=%fused_computation.178 | loop fusion | bytes 12582912 | tf_op jit(solution)/shard_map/slice | solution.py:21
  170.6 4.7 %copy.48 = bf16[1024,1536]{0,1:T(8,128)(2,1)} copy(bf16[1024,1536]{1,0:T(8,128)(2,1)} %get-tuple-element.6) | data formatting | bytes 6291456 | tf_op jit(solution)/shard_map/slice | solution.py:21
  175.3 1.7 fusion
  177.0 0.9 copy.80
  177.9 4.3 %all-to-all-start.1 = ((bf16[8,256,128]{2,1,0:T(8,128)(2,1)}), bf16[8,256,128]{2,1,0:T(8,128)(2,1)}, u32[]{:S(2)}, u32[]{:S(2)}) async-start(bf16[8,256,128]{2,1,0:T(8,128)(2,1)} %bitcast.89), calls=%async_computation.1 | async-start | bytes 1048576 | tf_op jit(solution)/shard_map/all_to_all | solution.py:43
  183.3 0.6 fusion.81
  183.9 8.7 %all-to-all-done.1 = bf16[8,256,128]{2,1,0:T(8,128)(2,1)} async-done(((bf16[8,256,128]{2,1,0:T(8,128)(2,1)}), bf16[8,256,128]{2,1,0:T(8,128)(2,1)}, u32[]{:S(2)}, u32[]{:S(2)}) %all-to-all-start.1) | async-done | bytes 524320 | tf_op jit(solution)/shard_map/all_to_all | solution.py:43
  192.6 1.1 reduce_sum.92
  193.7 2.4 collective-permute-start
  196.1 0.7 fusion.75
  196.8 4.6 %collective-permute-done = bf16[16,128]{1,0:T(8,128)(2,1)S(1)} collective-permute-done((bf16[16,128]{1,0:T(8,128)(2,1)S(1)}, bf16[16,128]{1,0:T(8,128)(2,1)S(1)}, u32[]{:S(2)}, u32[]{:S(2)}) %collective-permute-start) | collective-permute-done | bytes 4128 | tf_op jit(solution)/shard_map/ppermute | solution.py:50
  201.5 1.0 fusion.72
  202.6 0.8 broadcast_in_dim.275
  203.4 4.2 %all-to-all-start.2 = ((bf16[8,256,128]{1,2,0:T(8,128)(2,1)}), bf16[8,256,128]{1,2,0:T(8,128)(2,1)}, u32[]{:S(2)}, u32[]{:S(2)}) async-start(bf16[8,256,128]{1,2,0:T(8,128)(2,1)} %broadcast_in_dim.275), calls=%async_computation.2 | async-start | bytes 1048576 | tf_op jit(solution)/shard_map/all_to_all | solution.py:29
  207.5 2.9 copy.52
  210.5 7.4 %all-to-all-done.2 = bf16[8,256,128]{1,2,0:T(8,128)(2,1)} async-done(((bf16[8,256,128]{1,2,0:T(8,128)(2,1)}), bf16[8,256,128]{1,2,0:T(8,128)(2,1)}, u32[]{:S(2)}, u32[]{:S(2)}) %all-to-all-start.2) | async-done | bytes 524320 | tf_op jit(solution)/shard_map/all_to_all | solution.py:29
  217.9 2.0 multiply_reduce_fusion.1
  220.6 3.3 %all-to-all-start.3 = ((f32[8,1,256]{2,1,0:T(1,128)}), f32[8,1,256]{2,1,0:T(1,128)S(1)}, u32[]{:S(2)}, u32[]{:S(2)}) async-start(f32[8,1,256]{2,1,0:T(1,128)} %broadcast_in_dim.276), calls=%async_computation.3 | async-start | bytes 16384 | tf_op jit(solution)/shard_map/all_to_all | solution.py:29
  224.0 0.7 constant_dynamic-slice_fusion.3
  224.6 4.5 %all-to-all-done.3 = f32[8,1,256]{2,1,0:T(1,128)S(1)} async-done(((f32[8,1,256]{2,1,0:T(1,128)}), f32[8,1,256]{2,1,0:T(1,128)S(1)}, u32[]{:S(2)}, u32[]{:S(2)}) %all-to-all-start.3) | async-done | bytes 8224 | tf_op jit(solution)/shard_map/all_to_all | solution.py:29
  229.2 1.7 fusion.1
  231.1 13.7 %all_to_all.48 = bf16[8,256,128]{2,1,0:T(8,128)(2,1)} all-to-all(bf16[8,256,128]{2,1,0:T(8,128)(2,1)S(1)} %bitcast.90), channel_id=1, replica_groups=mesh['sp'=64,'tp'=8] {'tp'}, dimensions={0} | all-to-all | bytes 1048576 | tf_op jit(solution)/shard_map/all_to_all | solution.py:43
  244.8 1.1 reduce_sum.95
  245.9 1.9 collective-permute-start.1
  247.8 0.7 fusion.76
  248.5 5.0 %collective-permute-done.1 = bf16[16,128]{1,0:T(8,128)(2,1)S(1)} collective-permute-done((bf16[16,128]{1,0:T(8,128)(2,1)S(1)}, bf16[16,128]{1,0:T(8,128)(2,1)S(1)}, u32[]{:S(2)}, u32[]{:S(2)}) %collective-permute-start.1) | collective-permute-done | bytes 4128 | tf_op jit(solution)/shard_map/ppermute | solution.py:50
  254.2 12.8 %all_to_all.49 = bf16[8,256,128]{1,2,0:T(8,128)(2,1)S(1)} all-to-all(bf16[8,256,128]{1,2,0:T(8,128)(2,1)S(1)} %broadcast_in_dim.277), channel_id=1, replica_groups=mesh['sp'=64,'tp'=8] {'tp'}, dimensions={0} | all-to-all | bytes 1048576 | tf_op jit(solution)/shard_map/all_to_all | solution.py:29
  267.0 2.3 multiply_reduce_fusion
  269.3 0.6 broadcast_in_dim.278
  269.9 3.3 %all-to-all-start.6 = ((f32[8,1,256]{2,1,0:T(1,128)}), f32[8,1,256]{2,1,0:T(1,128)S(1)}, u32[]{:S(2)}, u32[]{:S(2)}) async-start(f32[8,1,256]{2,1,0:T(1,128)} %broadcast_in_dim.278), calls=%async_computation.6 | async-start | bytes 16384 | tf_op jit(solution)/shard_map/all_to_all | solution.py:29
  273.2 5.2 %all-to-all-done.6 = f32[8,1,256]{2,1,0:T(1,128)S(1)} async-done(((f32[8,1,256]{2,1,0:T(1,128)}), f32[8,1,256]{2,1,0:T(1,128)S(1)}, u32[]{:S(2)}, u32[]{:S(2)}) %all-to-all-start.6) | async-done | bytes 8224 | tf_op jit(solution)/shard_map/all_to_all | solution.py:29
  278.5 1.9 fusion.2
  280.5 13.4 %all_to_all.50 = bf16[8,256,128]{2,1,0:T(8,128)(2,1)} all-to-all(bf16[8,256,128]{2,1,0:T(8,128)(2,1)S(1)} %bitcast.91), channel_id=1, replica_groups=mesh['sp'=64,'tp'=8] {'tp'}, dimensions={0} | all-to-all | bytes 1048576 | tf_op jit(solution)/shard_map/all_to_all | solution.py:43
  294.0 1.1 reduce_sum.98
  295.1 1.9 collective-permute-start.2
  297.0 0.6 fusion.77
  297.6 5.1 %collective-permute-done.2 = bf16[16,128]{1,0:T(8,128)(2,1)S(1)} collective-permute-done((bf16[16,128]{1,0:T(8,128)(2,1)S(1)}, bf16[16,128]{1,0:T(8,128)(2,1)S(1)}, u32[]{:S(2)}, u32[]{:S(2)}) %collective-permute-start.2) | collective-permute-done | bytes 4128 | tf_op jit(solution)/shard_map/ppermute | solution.py:50
  303.2 12.8 %all_to_all.51 = bf16[8,256,128]{1,2,0:T(8,128)(2,1)S(1)} all-to-all(bf16[8,256,128]{1,2,0:T(8,128)(2,1)S(1)} %broadcast_in_dim.279), channel_id=1, replica_groups=mesh['sp'=64,'tp'=8] {'tp'}, dimensions={0} | all-to-all | bytes 1048576 | tf_op jit(solution)/shard_map/all_to_all | solution.py:29
  315.9 2.2 fusion.5
  (104 shorter events, 4.4 us)
Async XLA Ops:
  6.5 159.1 %all-gather.2.cloned.1.call-start = ((), (), s32[]{:S(2)}) async-start(), calls=%async_computation.9 | async-start | bytes 6389760 | tf_op jit(solution)/shard_map/all_gather | solution.py:19
  10.5 9.6 %all-to-all-start = ((f32[8,1,256]{2,1,0:T(1,128)}), f32[8,1,256]{2,1,0:T(1,128)S(1)}, u32[]{:S(2)}, u32[]{:S(2)}) async-start(f32[8,1,256]{2,1,0:T(1,128)} %broadcast_in_dim.258), calls=%async_computation | async-start | bytes 16384 | tf_op jit(solution)/shard_map/all_to_all | solution.py:29
  14.8 186.5 %copy-start.6 = (pred[128]{0:T(512)(128)(4,1)}, pred[128]{0:T(512)(128)(4,1)S(1)}, u32[]{:S(2)}) copy-start(pred[128]{0:T(512)(128)(4,1)S(1)} %get-tuple-element.17) | copy-start | bytes 388
  14.8 186.5 %copy-start.8 = (pred[128]{0:T(512)(128)(4,1)}, pred[128]{0:T(512)(128)(4,1)S(1)}, u32[]{:S(2)}) copy-start(pred[128]{0:T(512)(128)(4,1)S(1)} %get-tuple-element.18) | copy-start | bytes 388
  14.9 186.5 %copy-start.10 = (pred[128]{0:T(512)(128)(4,1)}, pred[128]{0:T(512)(128)(4,1)S(1)}, u32[]{:S(2)}) copy-start(pred[128]{0:T(512)(128)(4,1)S(1)} %get-tuple-element.19) | copy-start | bytes 388
  14.9 186.5 %copy-start.12 = (pred[128]{0:T(512)(128)(4,1)}, pred[128]{0:T(512)(128)(4,1)S(1)}, u32[]{:S(2)}) copy-start(pred[128]{0:T(512)(128)(4,1)S(1)} %get-tuple-element.20) | copy-start | bytes 388
  14.9 186.5 %copy-start.14 = (pred[128]{0:T(512)(128)(4,1)}, pred[128]{0:T(512)(128)(4,1)S(1)}, u32[]{:S(2)}) copy-start(pred[128]{0:T(512)(128)(4,1)S(1)} %get-tuple-element.21) | copy-start | bytes 388
  14.9 186.5 %copy-start.16 = (pred[128]{0:T(512)(128)(4,1)}, pred[128]{0:T(512)(128)(4,1)S(1)}, u32[]{:S(2)}) copy-start(pred[128]{0:T(512)(128)(4,1)S(1)} %get-tuple-element.22) | copy-start | bytes 388
  14.9 186.5 %copy-start.18 = (pred[128]{0:T(512)(128)(4,1)}, pred[128]{0:T(512)(128)(4,1)S(1)}, u32[]{:S(2)}) copy-start(pred[128]{0:T(512)(128)(4,1)S(1)} %get-tuple-element.23) | copy-start | bytes 388
  14.9 186.5 %copy-start.20 = (pred[128]{0:T(512)(128)(4,1)}, pred[128]{0:T(512)(128)(4,1)S(1)}, u32[]{:S(2)}) copy-start(pred[128]{0:T(512)(128)(4,1)S(1)} %get-tuple-element.24) | copy-start | bytes 388
  15.0 186.4 %copy-start.22 = (pred[128]{0:T(512)(128)(4,1)}, pred[128]{0:T(512)(128)(4,1)S(1)}, u32[]{:S(2)}) copy-start(pred[128]{0:T(512)(128)(4,1)S(1)} %get-tuple-element.29) | copy-start | bytes 388
  15.0 186.4 %copy-start.24 = (pred[128]{0:T(512)(128)(4,1)}, pred[128]{0:T(512)(128)(4,1)S(1)}, u32[]{:S(2)}) copy-start(pred[128]{0:T(512)(128)(4,1)S(1)} %get-tuple-element.30) | copy-start | bytes 388
  15.5 185.9 %copy-start.26 = (pred[128]{0:T(512)(128)(4,1)}, pred[128]{0:T(512)(128)(4,1)S(1)}, u32[]{:S(2)}) copy-start(pred[128]{0:T(512)(128)(4,1)S(1)} %get-tuple-element.25) | copy-start | bytes 388
  170.6 4.7 %copy-start.2 = (bf16[256,512]{1,0:T(8,128)(2,1)S(1)}, bf16[256,512]{1,0:T(8,128)(2,1)}, u32[]{:S(2)}) copy-start(bf16[256,512]{1,0:T(8,128)(2,1)} %param.5) | copy-start | bytes 786436
  175.2 8.0 %copy-start.5 = (f32[3,1024]{1,0:T(4,128)S(1)}, f32[3,1024]{1,0:T(4,128)}, u32[]{:S(2)}) copy-start(f32[3,1024]{1,0:T(4,128)} %param.8) | copy-start | bytes 36868
  177.9 14.7 %all-to-all-start.1 = ((bf16[8,256,128]{2,1,0:T(8,128)(2,1)}), bf16[8,256,128]{2,1,0:T(8,128)(2,1)}, u32[]{:S(2)}, u32[]{:S(2)}) async-start(bf16[8,256,128]{2,1,0:T(8,128)(2,1)} %bitcast.89), calls=%async_computation.1 | async-start | bytes 1048576 | tf_op jit(solution)/shard_map/all_to_all | solution.py:43
  183.3 18.2 %copy-start.3 = (s32[256]{0:T(256)}, s32[256]{0:T(256)S(1)}, u32[]{:S(2)}) copy-start(s32[256]{0:T(256)S(1)} %add_add_fusion) | copy-start | bytes 3076
  193.7 7.6 %collective-permute-start = (bf16[16,128]{1,0:T(8,128)(2,1)S(1)}, bf16[16,128]{1,0:T(8,128)(2,1)S(1)}, u32[]{:S(2)}, u32[]{:S(2)}) collective-permute-start(bf16[16,128]{1,0:T(8,128)(2,1)S(1)} %slice.265), channel_id=1, source_target_pairs={{0,8},{8,16},{16,24},{24,32},{32,40},{40,48},{48,56},{56,64},{64,7... | collective-permute-start | bytes 12296 | tf_op jit(solution)/shard_map/ppermute | solution.py:50
  203.4 14.5 %all-to-all-start.2 = ((bf16[8,256,128]{1,2,0:T(8,128)(2,1)}), bf16[8,256,128]{1,2,0:T(8,128)(2,1)}, u32[]{:S(2)}, u32[]{:S(2)}) async-start(bf16[8,256,128]{1,2,0:T(8,128)(2,1)} %broadcast_in_dim.275), calls=%async_computation.2 | async-start | bytes 1048576 | tf_op jit(solution)/shard_map/all_to_all | solution.py:29
  219.8 11.1 %copy-start.1 = (f32[256,512]{1,0:T(8,128)}, f32[256,512]{1,0:T(8,128)S(1)}, u32[]{:S(2)}) copy-start(f32[256,512]{1,0:T(8,128)S(1)} %get-tuple-element.14) | copy-start | bytes 1572868
  219.8 33.7 %copy-start.4 = (s32[256]{0:T(256)S(1)}, s32[256]{0:T(256)}, u32[]{:S(2)}) copy-start(s32[256]{0:T(256)} %copy-done.3) | copy-start | bytes 3076
  219.8 33.7 %copy-start.7 = (pred[128]{0:T(512)(128)(4,1)S(1)}, pred[128]{0:T(512)(128)(4,1)}, u32[]{:S(2)}) copy-start(pred[128]{0:T(512)(128)(4,1)} %copy-done.6) | copy-start | bytes 388
  219.8 33.7 %copy-start.9 = (pred[128]{0:T(512)(128)(4,1)S(1)}, pred[128]{0:T(512)(128)(4,1)}, u32[]{:S(2)}) copy-start(pred[128]{0:T(512)(128)(4,1)} %copy-done.8) | copy-start | bytes 388
  219.9 33.7 %copy-start.11 = (pred[128]{0:T(512)(128)(4,1)S(1)}, pred[128]{0:T(512)(128)(4,1)}, u32[]{:S(2)}) copy-start(pred[128]{0:T(512)(128)(4,1)} %copy-done.10) | copy-start | bytes 388
  219.9 33.7 %copy-start.13 = (pred[128]{0:T(512)(128)(4,1)S(1)}, pred[128]{0:T(512)(128)(4,1)}, u32[]{:S(2)}) copy-start(pred[128]{0:T(512)(128)(4,1)} %copy-done.12) | copy-start | bytes 388
  219.9 33.7 %copy-start.15 = (pred[128]{0:T(512)(128)(4,1)S(1)}, pred[128]{0:T(512)(128)(4,1)}, u32[]{:S(2)}) copy-start(pred[128]{0:T(512)(128)(4,1)} %copy-done.14) | copy-start | bytes 388
  219.9 33.7 %copy-start.17 = (pred[128]{0:T(512)(128)(4,1)S(1)}, pred[128]{0:T(512)(128)(4,1)}, u32[]{:S(2)}) copy-start(pred[128]{0:T(512)(128)(4,1)} %copy-done.16) | copy-start | bytes 388
  219.9 33.7 %copy-start.19 = (pred[128]{0:T(512)(128)(4,1)S(1)}, pred[128]{0:T(512)(128)(4,1)}, u32[]{:S(2)}) copy-start(pred[128]{0:T(512)(128)(4,1)} %copy-done.18) | copy-start | bytes 388
  219.9 33.7 %copy-start.21 = (pred[128]{0:T(512)(128)(4,1)S(1)}, pred[128]{0:T(512)(128)(4,1)}, u32[]{:S(2)}) copy-start(pred[128]{0:T(512)(128)(4,1)} %copy-done.20) | copy-start | bytes 388
  219.9 33.7 %copy-start.23 = (pred[128]{0:T(512)(128)(4,1)S(1)}, pred[128]{0:T(512)(128)(4,1)}, u32[]{:S(2)}) copy-start(pred[128]{0:T(512)(128)(4,1)} %copy-done.22) | copy-start | bytes 388
  219.9 33.7 %copy-start.25 = (pred[128]{0:T(512)(128)(4,1)S(1)}, pred[128]{0:T(512)(128)(4,1)}, u32[]{:S(2)}) copy-start(pred[128]{0:T(512)(128)(4,1)} %copy-done.24) | copy-start | bytes 388
  219.9 33.7 %copy-start.27 = (pred[128]{0:T(512)(128)(4,1)S(1)}, pred[128]{0:T(512)(128)(4,1)}, u32[]{:S(2)}) copy-start(pred[128]{0:T(512)(128)(4,1)} %copy-done.26) | copy-start | bytes 388
  219.9 33.7 %copy-start.28 = (pred[128]{0:T(512)(128)(4,1)S(1)}, pred[128]{0:T(512)(128)(4,1)}, u32[]{:S(2)}) copy-start(pred[128]{0:T(512)(128)(4,1)} %get-tuple-element.26) | copy-start | bytes 388
  220.0 33.7 %copy-start.29 = (pred[128]{0:T(512)(128)(4,1)S(1)}, pred[128]{0:T(512)(128)(4,1)}, u32[]{:S(2)}) copy-start(pred[128]{0:T(512)(128)(4,1)} %get-tuple-element.27) | copy-start | bytes 388
  220.0 33.7 %copy-start.30 = (pred[128]{0:T(512)(128)(4,1)S(1)}, pred[128]{0:T(512)(128)(4,1)}, u32[]{:S(2)}) copy-start(pred[128]{0:T(512)(128)(4,1)} %get-tuple-element.28) | copy-start | bytes 388
  220.0 33.7 %copy-start.31 = (s32[128]{0:T(128)S(1)}, s32[128]{0:T(128)}, u32[]{:S(2)}) copy-start(s32[128]{0:T(128)} %fusion.78) | copy-start | bytes 1540
  220.0 33.7 %copy-start.32 = (pred[128]{0:T(512)(128)(4,1)S(1)}, pred[128]{0:T(512)(128)(4,1)}, u32[]{:S(2)}) copy-start(pred[128]{0:T(512)(128)(4,1)} %get-tuple-element.31) | copy-start | bytes 388
  220.0 33.7 %copy-start.33 = (pred[128]{0:T(512)(128)(4,1)S(1)}, pred[128]{0:T(512)(128)(4,1)}, u32[]{:S(2)}) copy-start(pred[128]{0:T(512)(128)(4,1)} %get-tuple-element.32) | copy-start | bytes 388
  220.6 8.6 %all-to-all-start.3 = ((f32[8,1,256]{2,1,0:T(1,128)}), f32[8,1,256]{2,1,0:T(1,128)S(1)}, u32[]{:S(2)}, u32[]{:S(2)}) async-start(f32[8,1,256]{2,1,0:T(1,128)} %broadcast_in_dim.276), calls=%async_computation.3 | async-start | bytes 16384 | tf_op jit(solution)/shard_map/all_to_all | solution.py:29
  231.1 35.9 %copy-start = (bf16[1024,1536]{0,1:T(8,128)(2,1)S(1)}, bf16[1024,1536]{0,1:T(8,128)(2,1)}, u32[]{:S(2)}) copy-start(bf16[1024,1536]{0,1:T(8,128)(2,1)} %copy.52) | copy-start | bytes 9437188
  245.9 7.6 %collective-permute-start.1 = (bf16[16,128]{1,0:T(8,128)(2,1)S(1)}, bf16[16,128]{1,0:T(8,128)(2,1)S(1)}, u32[]{:S(2)}, u32[]{:S(2)}) collective-permute-start(bf16[16,128]{1,0:T(8,128)(2,1)S(1)} %slice.285), channel_id=1, source_target_pairs={{0,8},{8,16},{16,24},{24,32},{32,40},{40,48},{48,56},{56,64},{64,7... | collective-permute-start | bytes 12296 | tf_op jit(solution)/shard_map/ppermute | solution.py:50
  269.9 8.6 %all-to-all-start.6 = ((f32[8,1,256]{2,1,0:T(1,128)}), f32[8,1,256]{2,1,0:T(1,128)S(1)}, u32[]{:S(2)}, u32[]{:S(2)}) async-start(f32[8,1,256]{2,1,0:T(1,128)} %broadcast_in_dim.278), calls=%async_computation.6 | async-start | bytes 16384 | tf_op jit(solution)/shard_map/all_to_all | solution.py:29
  295.1 7.6 %collective-permute-start.2 = (bf16[16,128]{1,0:T(8,128)(2,1)S(1)}, bf16[16,128]{1,0:T(8,128)(2,1)S(1)}, u32[]{:S(2)}, u32[]{:S(2)}) collective-permute-start(bf16[16,128]{1,0:T(8,128)(2,1)S(1)} %slice.304), channel_id=1, source_target_pairs={{0,8},{8,16},{16,24},{24,32},{32,40},{40,48},{48,56},{56,64},{64,7... | collective-permute-start | bytes 12296 | tf_op jit(solution)/shard_map/ppermute | solution.py:50
Sparse Core Ops, SparseCore 0:
  10.3 155.2 all-gather.1
where the time goes:
time: 326 us; the launch traced here: 325 us
  waiting for transfers between devices  188 us (58%)
  blocking collectives  52.7 us (16%)
  starting transfers between devices  25.6 us (8%)
  local copies, waits for them, and re-layouts  23.3 us (7%)
  between operations  14.1 us (4%)
  matrix products  11.8 us (4%)
  other arithmetic  9.07 us (3%)
    all_gather x1, waiting for transfers between devices, turned_gather(): lax.all_gather(both, axis, axis=0, tiled=True)  145 us
    all_to_all x2, blocking collectives, summed_on_arrival(): lax.all_to_all(parts, axis, split_axis=0, concat_axis=0, tiled=True)  27.2 us
    all_to_all x2, blocking collectives, copy_for_each(): return lax.all_to_all(copies, axis, split_axis=0, concat_axis=0, tiled=True)  25.5 us
    all_to_all x4, waiting for transfers between devices, copy_for_each(): return lax.all_to_all(copies, axis, split_axis=0, concat_axis=0, tiled=True)  19.6 us
    all_to_all x4, starting transfers between devices, copy_for_each(): return lax.all_to_all(copies, axis, split_axis=0, concat_axis=0, tiled=True)  15.1 us
    ppermute x3, waiting for transfers between devices, from_behind(): lax.ppermute(value, axis, [(source, source + steps) for source in range(i...  14.6 us
    slice x3, local copies, waits for them, and re-layouts, turned_gather(): section = filled[:, at:at + t[0].size].reshape(-1, *t.shape[1:])  12.6 us
    all_to_all x1, waiting for transfers between devices, summed_on_arrival(): lax.all_to_all(parts, axis, split_axis=0, concat_axis=0, tiled=True)  8.71 us
  transfers between devices with their start and end apart: 9, of which 9 were waited for; matrix products, arithmetic and copies ran while one was open for 4% of the time, Pallas kernels for 0%

commit v1 on v0

v1 whole, which is shorter than its diff:
```python
import functools

import jax
import jax.numpy as jnp
from jax import lax
from jax.experimental import pallas as pl
from jax.experimental.pallas import tpu as pltpu
from jax.sharding import PartitionSpec as P

D = 4096
P_SIZE = 1024
LAYERS = 3
EPS = 1e-06
HALO = 16
NZ, NY, NT = 16, 4, 8
MESH = pl.DeviceIdType.MESH
BF16, F32 = jnp.bfloat16, jnp.float32


def remote(src, dst, send, recv, sp, tp):
    return pltpu.make_async_remote_copy(
        src_ref=src, dst_ref=dst, send_sem=send, recv_sem=recv,
        device_id=(sp, tp), device_id_type=MESH,
    )


def kernel(
    x_ref, gain_ref, win_ref, scale_ref, wout_ref, out_ref,
    wi, wo, state, part, rs_in, ssq, mixed, mix_in, tail, halo,
    z_send, z_recv, y_send, y_recv, rs_send, rs_recv,
    sq_send, sq_recv, mx_send, mx_recv, h_send, h_recv, own_sem,
):
    sp = lax.axis_index("sp")
    t = lax.axis_index("tp")
    z, y = sp // NY, sp % NY

    def at(zz, yy):
        return ((zz + NZ) % NZ) * NY + (yy + NY) % NY

    z_up, z_down = at(z + 1, y), at(z - 1, y)
    y_up, y_down = at(z, y + 1), at(z, y - 1)
    sp_next, sp_prev = (sp + 1) % (NZ * NY), (sp + NZ * NY - 1) % (NZ * NY)

    barrier = pltpu.get_barrier_semaphore()
    for peer in (z_up, z_down, y_up, y_down, sp_next, sp_prev):
        pl.semaphore_signal(barrier, inc=1, device_id=(peer, t), device_id_type=MESH)
    for d in range(1, NT):
        pl.semaphore_signal(
            barrier, inc=1, device_id=(sp, (t + d) % NT), device_id_type=MESH
        )

    own = []
    for layer in range(LAYERS):
        own.append(pltpu.make_async_copy(win_ref.at[layer], wi.at[layer, z, y], own_sem.at[2 * layer]))
        own.append(pltpu.make_async_copy(wout_ref.at[layer], wo.at[layer, z, y], own_sem.at[2 * layer + 1]))
    for copy in own:
        copy.start()
    for copy in own:
        copy.wait()
    pl.semaphore_wait(barrier, 6 + NT - 1)

    sent = []

    def go(copy):
        copy.start()
        sent.append(copy)
        return copy

    def piece_of(p):
        layer, kind = p // 2, p % 2
        return (wo if kind else wi).at[layer]

    def z_copy(p, direction, step, whole):
        buf = piece_of(p)
        block = (z - step + NZ) % NZ if direction == 0 else (z + step) % NZ
        ref = buf.at[block] if whole else buf.at[block, y]
        return remote(
            ref, ref, z_send.at[p, direction, step], z_recv.at[p, direction, step],
            z_up if direction == 0 else z_down, t,
        )

    def z_wait(p, direction, step, whole):
        z_copy(p, direction, step, whole).wait_recv()

    def y_copy(p, slot, whole):
        buf = piece_of(p)
        up = (y + 1) % NY
        down = (y + NY - 1) % NY
        if whole:
            refs = (buf.at[:, y], buf.at[:, y], buf.at[pl.ds(0, 8), down], buf.at[pl.ds(8, 8), up])
        else:
            half = 256
            refs = (
                buf.at[z, y], buf.at[z, y],
                buf.at[z, down, :, pl.ds(0, half)], buf.at[z, up, :, pl.ds(half, half)],
            )
        ref = refs[slot]
        return remote(
            ref, ref, y_send.at[p, slot], y_recv.at[p, slot], y_up if slot % 2 == 0 else y_down, t
        )

    def stage(p, k):
        z_first = p % 3 != 2
        if z_first:
            if 1 <= k <= 8:
                z_wait(p, 0, k - 1, False)
            if 1 <= k <= 7:
                z_wait(p, 1, k - 1, False)
            if k <= 7:
                go(z_copy(p, 0, k, False))
            if k <= 6:
                go(z_copy(p, 1, k, False))
            y0, whole = 8, True
        else:
            s = k - 2
            y0, whole = 0, False
        if k == y0:
            go(y_copy(p, 0, whole))
            go(y_copy(p, 1, whole))
        if k == y0 + 1:
            y_copy(p, 0, whole).wait_recv()
            y_copy(p, 1, whole).wait_recv()
            go(y_copy(p, 2, whole))
            go(y_copy(p, 3, whole))
        if k == y0 + 2:
            y_copy(p, 2, whole).wait_recv()
            y_copy(p, 3, whole).wait_recv()
        if not z_first:
            if 1 <= s <= 8:
                z_wait(p, 0, s - 1, True)
            if 1 <= s <= 7:
                z_wait(p, 1, s - 1, True)
            if 0 <= s <= 7:
                go(z_copy(p, 0, s, True))
            if 0 <= s <= 6:
                go(z_copy(p, 1, s, True))

    for k in range(11):
        for p in range(2 * LAYERS):
            stage(p, k)

    lane0 = t * (D // NT)
    state[...] = x_ref[...]
    row = lax.broadcasted_iota(jnp.int32, (256, 128), 0)
    group = t // 2
    window = jnp.left_shift(jnp.int32(2), group)
    position = sp * 256 + row
    inverse = 1.0 / jnp.minimum(position + 1, window).astype(F32)

    for layer in range(LAYERS):
        wide = state[...].astype(F32)
        squares = jnp.sum(wide * wide, axis=1, keepdims=True)
        squares = jnp.broadcast_to(squares, (256, 128)).T[0:1, :]
        ssq[layer, t] = squares
        for d in range(1, NT):
            go(remote(
                ssq.at[layer, t], ssq.at[layer, t],
                sq_send.at[layer, d], sq_recv.at[layer, d], sp, (t + d) % NT,
            ))
        own_gain = gain_ref[pl.ds(layer, 1), pl.ds(pl.multiple_of(lane0, 128), D // NT)]
        scaled = (wide * own_gain).astype(BF16)
        weights = wi[layer].reshape(P_SIZE, D // NT)
        partial = lax.dot_general(
            scaled, weights, (((1,), (1,)), ((), ())), preferred_element_type=F32
        ).astype(BF16)
        for j in range(NT):
            part[layer, j] = partial[:, j * 128:(j + 1) * 128]
        for d in range(1, NT):
            j = (t + d) % NT
            go(remote(
                part.at[layer, j], rs_in.at[layer, d],
                rs_send.at[layer, d], rs_recv.at[layer, d], sp, j,
            ))
        total = part[layer, t].astype(F32)
        for d in range(1, NT):
            remote(
                ssq.at[layer, t], ssq.at[layer, t],
                sq_send.at[layer, d], sq_recv.at[layer, d], sp, t,
            ).wait_recv()
        all_squares = jnp.sum(ssq[layer], axis=0)
        inv_rms = lax.rsqrt(all_squares / D + EPS)
        inv_rms = jnp.broadcast_to(inv_rms, (128, 256)).T
        for d in range(1, NT):
            remote(
                part.at[layer, 0], rs_in.at[layer, d],
                rs_send.at[layer, d], rs_recv.at[layer, d], sp, t,
            ).wait_recv()
            total = total + rs_in[layer, d].astype(F32)
        pool_in = (total * inv_rms).astype(BF16)
        tail[layer] = pool_in[256 - HALO:]
        edge = go(remote(
            tail.at[layer], halo.at[layer], h_send.at[layer], h_recv.at[layer], sp_next, t
        ))
        pool_in = pool_in.astype(F32)
        edge.wait_recv()
        before = halo[layer].astype(F32) * (sp > 0).astype(F32)
        run = jnp.concatenate([before, pool_in], axis=0)
        picked = None
        for g in range(4):
            run = run + pltpu.roll(run, 1 << g, 0)
            picked = run if g == 0 else jnp.where(group >= g, run, picked)
        means = picked[HALO:] * inverse - pool_in
        own_scale = scale_ref[pl.ds(layer, 1), pl.ds(pl.multiple_of(t * 128, 128), 128)]
        mixed[layer] = (means * own_scale).astype(BF16)
        for d in range(1, NT):
            go(remote(
                mixed.at[layer], mix_in.at[layer, t],
                mx_send.at[layer, d], mx_recv.at[layer, d], sp, (t + d) % NT,
            ))
        mix_in[layer, t] = mixed[layer]
        for d in range(1, NT):
            remote(
                mixed.at[layer], mix_in.at[layer, t],
                mx_send.at[layer, d], mx_recv.at[layer, d], sp, t,
            ).wait_recv()
        pooled = jnp.concatenate([mix_in[layer, k] for k in range(NT)], axis=1)
        branch = jnp.dot(
            pooled, wo[layer].reshape(P_SIZE, D // NT), preferred_element_type=F32
        )
        state[...] = (wide + branch).astype(BF16)

    out_ref[...] = state[...]
    for copy in sent:
        copy.wait_send()


def body(inputs, norm_gain, in_weight, pool_scale, out_weight):
    rows, features = inputs.shape
    vmem = pl.BlockSpec(memory_space=pltpu.VMEM)
    dma = pltpu.SemaphoreType.DMA
    pieces = 2 * LAYERS
    gathered = pltpu.VMEM((LAYERS, NZ, NY, P_SIZE // 64, features), BF16)
    blocks = pltpu.VMEM((LAYERS, NT, rows, 128), BF16)
    return pl.pallas_call(
        kernel,
        out_shape=jax.ShapeDtypeStruct(inputs.shape, inputs.dtype),
        in_specs=[vmem] * 5,
        out_specs=vmem,
        scratch_shapes=[
            gathered, gathered,
            pltpu.VMEM((rows, features), BF16),
            blocks, blocks,
            pltpu.VMEM((LAYERS, NT, 1, rows), F32),
            pltpu.VMEM((LAYERS, rows, 128), BF16),
            blocks,
            pltpu.VMEM((LAYERS, HALO, 128), BF16),
            pltpu.VMEM((LAYERS, HALO, 128), BF16),
            dma((pieces, 2, 8)), dma((pieces, 2, 8)),
            dma((pieces, 4)), dma((pieces, 4)),
            dma((LAYERS, NT)), dma((LAYERS, NT)),
            dma((LAYERS, NT)), dma((LAYERS, NT)),
            dma((LAYERS, NT)), dma((LAYERS, NT)),
            dma((LAYERS,)), dma((LAYERS,)),
            dma((pieces,)),
        ],
        compiler_params=pltpu.CompilerParams(
            collective_id=0, has_side_effects=True, vmem_limit_bytes=40 * 1024 * 1024
        ),
        name="mixer",
    )(inputs, norm_gain, jnp.swapaxes(in_weight, 1, 2), pool_scale, out_weight)


def solution(mesh):
    placed = (P("sp", "tp"), P(), P(None, "tp", "sp"), P(), P(None, "sp", "tp"))
    return jax.shard_map(body, mesh=mesh, in_specs=placed, out_specs=P("sp", "tp"), check_vma=False)
```

time: 326 us -> 142 us (0.44)
  the two profiles are of different devices: /device:TPU:32 before, /device:TPU:1 now
where the time goes in v1:
time: 142 us; the launch traced here: 141 us
  Pallas kernels  137 us (96%)
  local copies, waits for them, and re-layouts  4.81 us (3%)
    pallas_call x1, Pallas kernels, body(): pl.pallas_call(kernel, out_shape=jax.ShapeDtypeStruct(inputs.shape, input...  137 us
    unnamed x11, local copies, waits for them, and re-layouts  4.81 us

profile of v1, /device:TPU:1, one launch (start us, length us, event | category | flops | bytes accessed | tf_op | source)
XLA Modules:
  0.0 141.4 jit_solution(6404714037910718168)
XLA Ops:
  0.0 0.0 copy-start
  0.0 0.9 copy-done
  1.0 0.0 copy-start.1
  1.0 0.8 copy-done.1
  1.8 0.0 copy-start.2
  1.8 0.8 copy-done.2
  2.6 0.0 copy-start.3
  2.6 0.8 copy-done.3
  3.4 0.0 copy-start.4
  3.4 0.7 copy-done.4
  4.1 136.6 %mixer.1 = bf16[256,512]{1,0:T(8,128)(2,1)S(1)} custom-call(bf16[256,512]{1,0:T(8,128)(2,1)S(1)} %copy-done, f32[3,4096]{1,0:T(4,128)S(1)} %copy-done.1, bf16[3,16,512]{2,1,0:T(8,128)(2,1)S(1)} %bitcast.1, f32[3,1024]{1,0:T(4,128)S(1)} %copy-done.4, bf16[3,16,512]{2,1,0:T(8,128)(2,1)S(1)} %copy-done.3), custom_call_target="tpu_custom_call" | custom-call | tf_op jit(solution)/shard_map/mixer/pallas_call | solution.py:234
  140.7 0.7 copy.7
Async XLA Ops:
  0.0 0.9 copy-start
  1.0 0.8 copy-start.1
  1.8 0.8 copy-start.2
  2.6 0.8 copy-start.3
  3.4 0.7 copy-start.4

commit v2 on v1

v2 whole, which is shorter than its diff:
```python
import functools

import jax
import jax.numpy as jnp
from jax import lax
from jax.experimental import pallas as pl
from jax.experimental.pallas import tpu as pltpu
from jax.sharding import PartitionSpec as P

D = 4096
P_SIZE = 1024
LAYERS = 3
EPS = 1e-06
HALO = 16
NZ, NY, NT = 16, 4, 8
MESH = pl.DeviceIdType.MESH
BF16, F32 = jnp.bfloat16, jnp.float32


VMEM_LIMIT = 60 * 1024 * 1024
OTHERS = (4, 5, 2, 3, 6, 7, 1)
RELAYS = ((-6, (2, 1, -1)), (6, (1, -1)), (-2, (2, 1, -1)), (2, (-2, -1, 1)))
FIRST = (2, -6, -2, 6)
LATER = (1, -1, 3, -3, 4, -4, 5, -5, 7, -7, 8)
PLAN = {
    "start": ((0, 0), (0, 1), (1, 0), (0, 2), (1, 1), (2, 0), (0, 3), (1, 2), (2, 1), (0, 4)),
    ("b", 0): ((1, 3), (2, 2), (3, 0)),
    ("c", 0): ((2, 3), (3, 1), (4, 0)),
    ("d", 0): ((1, 4),),
    ("a", 1): ((2, 4),),
    ("b", 1): ((3, 2), (4, 1), (5, 0), (3, 3), (4, 2), (5, 1)),
    ("c", 1): ((4, 3), (5, 2)),
    ("d", 1): ((3, 4),),
    ("a", 2): ((4, 4),),
    ("b", 2): ((5, 3),),
    ("d", 2): ((5, 4),),
}


def remote(src, dst, send, recv, sp, tp):
    return pltpu.make_async_remote_copy(
        src_ref=src, dst_ref=dst, send_sem=send, recv_sem=recv,
        device_id=(sp, tp), device_id_type=MESH,
    )


def kernel(
    x_ref, gain_ref, win_ref, scale_ref, wout_ref, out_ref,
    wi, wo, state, gain, scale, part, rs_in, ssq, mixed, mix_in, tail, halo,
    z_send, z_recv, y_send, y_recv, rs_send, rs_recv,
    sq_send, sq_recv, mx_send, mx_recv, h_send, h_recv, own_sem,
):
    sp = lax.axis_index("sp")
    t = lax.axis_index("tp")
    z, y = sp // NY, sp % NY

    def at(zz, yy):
        return ((zz + NZ) % NZ) * NY + (yy + NY) % NY

    def peer(d):
        return ((t // 2 + d // 2) % 4) * 2 + (t + d) % 2

    sp_next, sp_prev = (sp + 1) % (NZ * NY), (sp + NZ * NY - 1) % (NZ * NY)

    barrier = pltpu.get_barrier_semaphore()
    greeted = [at(z + o, y) for o in (1, -1, 2, -2, 6, -6)]
    greeted += [at(z, y + 1), at(z, y - 1), sp_next, sp_prev]
    for to in greeted:
        pl.semaphore_signal(barrier, inc=1, device_id=(to, t), device_id_type=MESH)
    for d in OTHERS:
        pl.semaphore_signal(barrier, inc=1, device_id=(sp, peer(d)), device_id_type=MESH)

    own = []
    for layer in range(LAYERS):
        own.append(pltpu.make_async_copy(win_ref.at[layer], wi.at[layer, z, y], own_sem.at[2 * layer]))
        own.append(pltpu.make_async_copy(wout_ref.at[layer], wo.at[layer, z, y], own_sem.at[2 * layer + 1]))
    own.append(pltpu.make_async_copy(x_ref, state, own_sem.at[6]))
    own.append(pltpu.make_async_copy(gain_ref, gain, own_sem.at[7]))
    own.append(pltpu.make_async_copy(scale_ref, scale, own_sem.at[8]))
    for copy in own:
        copy.start()
    for copy in own:
        copy.wait()
    pl.semaphore_wait(barrier, len(greeted) + NT - 1)

    sent = []

    def go(copy):
        copy.start()
        sent.append(copy)
        return copy

    def piece(p):
        return (wo if p % 2 else wi).at[p // 2]

    def line(offset):
        return (z + offset + 2 * NZ) % NZ

    def along_z(p, offset, way, slot):
        block = piece(p).at[line(offset), y]
        go(remote(block, block, z_send.at[p, slot], z_recv.at[p, slot], at(z + way, y), t))

    def along_y(p, offset, from_y, way, slot):
        block = piece(p).at[line(offset), (y + from_y + NY) % NY]
        go(remote(block, block, y_send.at[p, slot], y_recv.at[p, slot], at(z, y + way), t))

    def arrived(p, sems, slot, count):
        blocks = piece(p).at[pl.ds(0, count), 0]
        remote(blocks, blocks, sems[0].at[p, slot], sems[1].at[p, slot], sp, t).wait_recv()

    zs, ys = (z_send, z_recv), (y_send, y_recv)

    def stage(p, k):
        if k == 0:
            for way in (6, -6, 2, -2):
                along_z(p, 0, way, 0)
            for way in (1, -1):
                along_y(p, 0, 0, way, 0 if way > 0 else 1)
        if k == 1:
            arrived(p, zs, 0, 4)
            for offset, ways in RELAYS:
                for way in ways:
                    along_z(p, offset, way, 1)
            for way in (1, -1):
                for offset in FIRST:
                    along_y(p, offset, 0, way, 2 if way > 0 else 3)
        if k == 2:
            arrived(p, zs, 1, 11)
            for way in (1, -1):
                for offset in LATER:
                    along_y(p, offset, 0, way, 4 if way > 0 else 5)
            for slot in (0, 1):
                arrived(p, ys, slot, 1)
                arrived(p, ys, slot + 2, 4)
            for offset in (0, 2, -6):
                along_y(p, offset, -1, 1, 6)
            for offset in (-2, 6):
                along_y(p, offset, 1, -1, 7)
        if k == 3:
            arrived(p, ys, 4, 11)
            arrived(p, ys, 5, 11)
            for offset in LATER[:5]:
                along_y(p, offset, -1, 1, 8)
            for offset in LATER[5:]:
                along_y(p, offset, 1, -1, 9)
        if k == 4:
            for slot, count in ((6, 3), (7, 2), (8, 5), (9, 6)):
                arrived(p, ys, slot, count)

    def advance(stages):
        for p, k in stages:
            stage(p, k)

    advance(PLAN["start"])

    lane0 = t * (D // NT)
    row = lax.broadcasted_iota(jnp.int32, (256, 128), 0)
    group = t // 2
    window = jnp.left_shift(jnp.int32(2), group)
    position = sp * 256 + row
    inverse = 1.0 / jnp.minimum(position + 1, window).astype(F32)

    for layer in range(LAYERS):
        wide = state[...].astype(F32)
        squares = jnp.sum(wide * wide, axis=1, keepdims=True)
        squares = jnp.broadcast_to(squares, (256, 128)).T[0:1, :]
        ssq[layer, t] = squares
        for d in OTHERS:
            go(remote(
                ssq.at[layer, t], ssq.at[layer, t],
                sq_send.at[layer, d], sq_recv.at[layer, d], sp, peer(d),
            ))
        advance(PLAN.get(("a", layer), ()))
        own_gain = gain[pl.ds(layer, 1), pl.ds(pl.multiple_of(lane0, 128), D // NT)]
        scaled = (wide * own_gain).astype(BF16)
        weights = wi[layer].reshape(P_SIZE, D // NT)
        partial = lax.dot_general(
            scaled, weights, (((1,), (1,)), ((), ())), preferred_element_type=F32
        ).astype(BF16)
        for j in range(NT):
            part[layer, j] = partial[:, j * 128:(j + 1) * 128]
        for d in OTHERS:
            j = peer(d)
            go(remote(
                part.at[layer, j], rs_in.at[layer, d],
                rs_send.at[layer, d], rs_recv.at[layer, d], sp, j,
            ))
        advance(PLAN.get(("b", layer), ()))
        total = part[layer, t].astype(F32)
        for d in OTHERS:
            remote(
                ssq.at[layer, t], ssq.at[layer, t],
                sq_send.at[layer, d], sq_recv.at[layer, d], sp, t,
            ).wait_recv()
        all_squares = jnp.sum(ssq[layer], axis=0)
        inv_rms = lax.rsqrt(all_squares / D + EPS)
        inv_rms = jnp.broadcast_to(inv_rms, (128, 256)).T
        for d in OTHERS:
            remote(
                part.at[layer, 0], rs_in.at[layer, d],
                rs_send.at[layer, d], rs_recv.at[layer, d], sp, t,
            ).wait_recv()
            total = total + rs_in[layer, d].astype(F32)
        pool_in = (total * inv_rms).astype(BF16)
        tail[layer] = pool_in[256 - HALO:]
        edge = go(remote(
            tail.at[layer], halo.at[layer], h_send.at[layer], h_recv.at[layer], sp_next, t
        ))
        pool_in = pool_in.astype(F32)
        edge.wait_recv()
        before = halo[layer].astype(F32) * (sp > 0).astype(F32)
        run = jnp.concatenate([before, pool_in], axis=0)
        picked = None
        for g in range(4):
            run = run + pltpu.roll(run, 1 << g, 0)
            picked = run if g == 0 else jnp.where(group >= g, run, picked)
        means = picked[HALO:] * inverse - pool_in
        own_scale = scale[pl.ds(layer, 1), pl.ds(pl.multiple_of(t * 128, 128), 128)]
        mixed[layer] = (means * own_scale).astype(BF16)
        for d in OTHERS:
            go(remote(
                mixed.at[layer], mix_in.at[layer, t],
                mx_send.at[layer, d], mx_recv.at[layer, d], sp, peer(d),
            ))
        mix_in[layer, t] = mixed[layer]
        advance(PLAN.get(("c", layer), ()))
        for d in OTHERS:
            remote(
                mixed.at[layer], mix_in.at[layer, t],
                mx_send.at[layer, d], mx_recv.at[layer, d], sp, t,
            ).wait_recv()
        advance(PLAN.get(("d", layer), ()))
        pooled = jnp.concatenate([mix_in[layer, k] for k in range(NT)], axis=1)
        branch = jnp.dot(
            pooled, wo[layer].reshape(P_SIZE, D // NT), preferred_element_type=F32
        )
        state[...] = (wide + branch).astype(BF16)

    out_ref[...] = state[...]
    for copy in sent:
        copy.wait_send()


def body(inputs, norm_gain, in_weight, pool_scale, out_weight):
    rows, features = inputs.shape
    vmem = pl.BlockSpec(memory_space=pltpu.VMEM)
    hbm = pl.BlockSpec(memory_space=pl.ANY)
    dma = pltpu.SemaphoreType.DMA
    pieces = 2 * LAYERS
    gathered = pltpu.VMEM((LAYERS, NZ, NY, P_SIZE // 64, features), BF16)
    blocks = pltpu.VMEM((LAYERS, NT, rows, 128), BF16)
    return pl.pallas_call(
        kernel,
        out_shape=jax.ShapeDtypeStruct(inputs.shape, inputs.dtype),
        in_specs=[hbm] * 5,
        out_specs=vmem,
        scratch_shapes=[
            gathered, gathered,
            pltpu.VMEM((rows, features), BF16),
            pltpu.VMEM(norm_gain.shape, F32),
            pltpu.VMEM(pool_scale.shape, F32),
            blocks, blocks,
            pltpu.VMEM((LAYERS, NT, 1, rows), F32),
            pltpu.VMEM((LAYERS, rows, 128), BF16),
            blocks,
            pltpu.VMEM((LAYERS, HALO, 128), BF16),
            pltpu.VMEM((LAYERS, HALO, 128), BF16),
            dma((pieces, 2)), dma((pieces, 2)),
            dma((pieces, 10)), dma((pieces, 10)),
            dma((LAYERS, NT)), dma((LAYERS, NT)),
            dma((LAYERS, NT)), dma((LAYERS, NT)),
            dma((LAYERS, NT)), dma((LAYERS, NT)),
            dma((LAYERS,)), dma((LAYERS,)),
            dma((pieces + 3,)),
        ],
        compiler_params=pltpu.CompilerParams(
            collective_id=0, has_side_effects=True, vmem_limit_bytes=VMEM_LIMIT
        ),
        name="mixer",
    )(inputs, norm_gain, jnp.swapaxes(in_weight, 1, 2), pool_scale, out_weight)


def solution(mesh):
    placed = (P("sp", "tp"), P(), P(None, "tp", "sp"), P(), P(None, "sp", "tp"))
    return jax.shard_map(body, mesh=mesh, in_specs=placed, out_specs=P("sp", "tp"), check_vma=False)
```

time: 142 us -> 107 us (0.75)
  Pallas kernels: 137 us -> 105 us
  local copies, waits for them, and re-layouts: 4.81 us -> 1.67 us
    pallas_call x1, Pallas kernels: 137 us -> 105 us  [body(): pl.pallas_call(kernel, out_shape=jax.ShapeDtypeStruct(inputs.shape, input...]
    unnamed x11 -> x1, local copies, waits for them, and re-layouts: 4.81 us -> 1.67 us
where the time goes in v2:
time: 107 us
  Pallas kernels  105 us (98%)
  local copies, waits for them, and re-layouts  1.67 us (2%)
    pallas_call x1, Pallas kernels, body(): pl.pallas_call(kernel, out_shape=jax.ShapeDtypeStruct(inputs.shape, input...  105 us

profile of v2, /device:TPU:1, one launch (start us, length us, event | category | flops | bytes accessed | tf_op | source)
XLA Modules:
  0.0 107.1 jit_solution(10682993933428744136)
XLA Ops:
  0.0 105.4 %mixer.1 = bf16[256,512]{1,0:T(8,128)(2,1)} custom-call(bf16[256,512]{1,0:T(8,128)(2,1)} %x_ref.1, f32[3,4096]{1,0:T(4,128)} %gain_ref.1, bf16[3,16,512]{2,1,0:T(8,128)(2,1)} %bitcast.1, f32[3,1024]{1,0:T(4,128)} %scale_ref.1, bf16[3,16,512]{2,1,0:T(8,128)(2,1)} %wout_ref.1), custom_call_target="tpu_custom_call" | custom-call | tf_op jit(solution)/shard_map/mixer/pallas_call | solution.py:252
  105.4 1.7 %copy.7 = bf16[256,512]{1,0:T(8,128)(2,1)} copy(bf16[256,512]{1,0:T(8,128)(2,1)} %mixer.1) | data formatting | bytes 524288

commit v3 on v2

v3 whole, which is shorter than its diff:
```python
import functools

import jax
import jax.numpy as jnp
from jax import lax
from jax.experimental import pallas as pl
from jax.experimental.pallas import tpu as pltpu
from jax.sharding import PartitionSpec as P

D = 4096
P_SIZE = 1024
LAYERS = 3
EPS = 1e-06
HALO = 16
AHEAD, SPLIT = 48, 112
NZ, NY, NT = 16, 4, 8
MESH = pl.DeviceIdType.MESH
BF16, F32 = jnp.bfloat16, jnp.float32


VMEM_LIMIT = 60 * 1024 * 1024
OTHERS = (4, 5, 2, 3, 6, 7, 1)
RELAYS = ((-6, (2, 1, -1)), (6, (1, -1)), (-2, (2, 1, -1)), (2, (-2, -1, 1)))
FIRST = (2, -6, -2, 6)
LATER = (1, -1, 3, -3, 4, -4, 5, -5, 7, -7, 8)
ROUND = (4, 5)
PLAN = {
    "start": (
        (0, 0), (4, 0), (5, 0), (1, 0), (0, 1), (4, 1), (5, 1), (2, 0), (1, 1),
        (0, 2), (4, 2), (3, 0), (0, 3), (2, 1), (1, 2), (5, 2), (4, 3), (0, 4),
    ),
    ("mid", 0): ((5, 3),),
    ("pool0", 0): ((3, 1), (4, 4), (1, 3), (2, 2)),
    ("pool1", 0): ((4, 5), (5, 4)),
    ("out0", 0): ((1, 4), (4, 6), (5, 5), (2, 3), (3, 2)),
    ("in0", 1): ((2, 4),),
    ("out1", 0): ((4, 7), (5, 6)),
    ("pool0", 1): ((3, 3), (4, 8), (5, 7)),
    ("pool1", 1): ((4, 9), (5, 8)),
    ("out0", 1): ((3, 4), (4, 10), (5, 9)),
    ("out1", 1): ((5, 10),),
}


def remote(src, dst, send, recv, sp, tp):
    return pltpu.make_async_remote_copy(
        src_ref=src, dst_ref=dst, send_sem=send, recv_sem=recv,
        device_id=(sp, tp), device_id_type=MESH,
    )


def kernel(
    x_ref, gain_ref, win_ref, scale_ref, wout_ref, out_ref,
    wi, wo, state, gain, scale, inverse, part, rs_in, ssq, mixed, mix_in,
    z_send, z_recv, y_send, y_recv, rs_send, rs_recv,
    sq_send, sq_recv, mx_send, mx_recv, h_send, h_recv, own_sem, r_recv,
):
    sp = lax.axis_index("sp")
    t = lax.axis_index("tp")
    z, y = sp // NY, sp % NY

    def at(zz, yy):
        return ((zz + NZ) % NZ) * NY + (yy + NY) % NY

    def peer(d):
        return ((t // 2 + d // 2) % 4) * 2 + (t + d) % 2

    sp_next, sp_prev = (sp + 1) % (NZ * NY), (sp + NZ * NY - 1) % (NZ * NY)

    barrier = pltpu.get_barrier_semaphore()
    greeted = [at(z + o, y) for o in (1, -1, 2, -2, 6, -6)]
    greeted += [at(z, y + 1), at(z, y - 1), sp_next, sp_prev]
    for to in greeted:
        pl.semaphore_signal(barrier, inc=1, device_id=(to, t), device_id_type=MESH)
    for d in OTHERS:
        pl.semaphore_signal(barrier, inc=1, device_id=(sp, peer(d)), device_id_type=MESH)

    own = []
    for layer in range(LAYERS):
        own.append(pltpu.make_async_copy(win_ref.at[layer], wi.at[layer, z, y], own_sem.at[0]))
        own.append(pltpu.make_async_copy(wout_ref.at[layer], wo.at[layer, z, y], own_sem.at[0]))
    own.append(pltpu.make_async_copy(x_ref, state.at[pl.ds(AHEAD, 256)], own_sem.at[1]))
    own.append(pltpu.make_async_copy(gain_ref, gain, own_sem.at[2]))
    own.append(pltpu.make_async_copy(scale_ref, scale, own_sem.at[3]))
    for copy in own:
        copy.start()
    six = wi.at[0, pl.ds(0, 2 * LAYERS), 0]
    pltpu.make_async_copy(six, six, own_sem.at[0]).wait()
    for copy in own[2 * LAYERS:]:
        copy.wait()
    pl.semaphore_wait(barrier, len(greeted) + NT - 1)

    def piece(p):
        return (wo if p % 2 else wi).at[p // 2]

    def line(offset):
        return (z + offset + 2 * NZ) % NZ

    def along_z(p, offset, way, slot):
        block = piece(p).at[line(offset), y]
        remote(block, block, z_send.at[p], z_recv.at[p, slot], at(z + way, y), t).start()

    def along_y(p, offset, from_y, way, slot):
        block = piece(p).at[line(offset), (y + from_y + NY) % NY]
        remote(block, block, y_send.at[p], y_recv.at[p, slot], at(z, y + way), t).start()

    def landed(blocks, sem):
        remote(blocks, blocks, sem, sem, sp, t).wait_recv()

    def stage(p, k):
        if k == 0:
            for way in (6, -6, 2, -2):
                along_z(p, 0, way, 0)
            for way in (1, -1):
                along_y(p, 0, 0, way, 0)
        if k == 1:
            landed(piece(p).at[pl.ds(0, 4), 0], z_recv.at[p, 0])
            for offset, ways in RELAYS:
                for way in ways:
                    along_z(p, offset, way, 1)
            for way in (1, -1):
                for offset in FIRST:
                    along_y(p, offset, 0, way, 0)
        if k == 2:
            landed(piece(p).at[pl.ds(0, 11), 0], z_recv.at[p, 1])
            for way in (1, -1):
                for offset in LATER:
                    along_y(p, offset, 0, way, 1)
            landed(piece(p).at[pl.ds(0, 5), pl.ds(0, 2)], y_recv.at[p, 0])
            for offset in (0, 2, -6):
                along_y(p, offset, -1, 1, 2)
            for offset in (-2, 6):
                along_y(p, offset, 1, -1, 2)
        if k == 3:
            landed(piece(p).at[pl.ds(0, 11), pl.ds(0, 2)], y_recv.at[p, 1])
            for offset in LATER[:5]:
                along_y(p, offset, -1, 1, 2)
            for offset in LATER[5:]:
                along_y(p, offset, 1, -1, 2)
        if k == 4:
            landed(piece(p).at[:, 0], y_recv.at[p, 2])

    def ring_copy(p, way, step):
        row = piece(p).at[line(-way * step)]
        remote(
            row, row, z_send.at[p], r_recv.at[p - ROUND[0], step], at(z + way, y), t
        ).start()

    def ring_stage(p, k):
        if k == 0:
            for way in (1, -1):
                along_y(p, 0, 0, way, 0)
        if k == 1:
            landed(piece(p).at[pl.ds(0, 2), 0], y_recv.at[p, 0])
            for way in (1, -1):
                half = piece(p).at[z, (y - way + NY) % NY, :, pl.ds(128 + 128 * way, 256)]
                remote(half, half, y_send.at[p], y_recv.at[p, 1], at(z, y + way), t).start()
        if k == 2:
            landed(piece(p).at[0, 0], y_recv.at[p, 1])
        if 3 <= k <= 10:
            landed(piece(p).at[pl.ds(0, 2 if k < 10 else 1)], r_recv.at[p - ROUND[0], k - 3])
        for way, steps in ((1, 8), (-1, 7)):
            if 2 <= k < 2 + steps:
                ring_copy(p, way, k - 2)

    def advance(*where):
        for p, k in PLAN.get(where[0] if len(where) == 1 else where, ()):
            if p in ROUND:
                ring_stage(p, k)
            else:
                stage(p, k)

    ahead = remote(
        x_ref.at[pl.ds(256 - AHEAD, AHEAD)], state.at[pl.ds(0, AHEAD)],
        h_send.at[0], h_recv.at[0], sp_next, t,
    )
    ahead.start()
    window = jnp.left_shift(jnp.int32(2), t // 2)
    position = sp * 256 - AHEAD + lax.broadcasted_iota(jnp.int32, inverse.shape, 0)
    count = jnp.maximum(jnp.minimum(position + 1, window), 1)
    inverse[...] = 1.0 / count.astype(F32)
    advance("start")
    ahead.wait_recv()
    first = state[0:AHEAD].astype(F32) * (sp > 0).astype(F32)
    state[0:AHEAD] = first.astype(BF16)

    lane0 = pl.multiple_of(t * (D // NT), 128)
    lane1 = pl.multiple_of(t * 128, 128)
    group = t // 2

    def rows_in(h, layer):
        return (HALO * layer, AHEAD + SPLIT - HALO * layer) if h == 0 else (AHEAD + SPLIT, 256 - SPLIT)

    def rows_out(h, layer):
        start, count = rows_in(h, layer)
        return (start, count) if h else (start + HALO, count - HALO)

    def part_copy(h, layer, d, j):
        rows = pl.ds(0, rows_in(h, layer)[1])
        return remote(
            part.at[layer, h, j, rows], rs_in.at[layer, h, d, rows],
            rs_send.at[layer, h], rs_recv.at[layer, h], sp, j,
        )

    def square_copy(h, layer, d, j):
        return remote(
            ssq.at[layer, h, t], ssq.at[layer, h, t],
            sq_send.at[layer, h], sq_recv.at[layer, h], sp, j,
        )

    def mixed_copy(h, layer, d, j):
        rows = pl.ds(0, rows_out(h, layer)[1])
        return remote(
            mixed.at[layer, h, rows], mix_in.at[layer, h, t, rows],
            mx_send.at[layer, h], mx_recv.at[layer, h], sp, j,
        )

    def project_in(h, layer):
        start, count = rows_in(h, layer)
        wide = state[start:start + count].astype(F32)
        squares = jnp.sum(wide * wide, axis=1, keepdims=True)
        squares = jnp.broadcast_to(squares, (count, 128))
        squares = jnp.concatenate([squares, jnp.zeros((256 - count, 128), F32)], axis=0)
        ssq[layer, h, t] = squares.T[0:1, :]
        for d in OTHERS:
            square_copy(h, layer, d, peer(d)).start()
        own_gain = gain[pl.ds(layer, 1), pl.ds(lane0, D // NT)]
        scaled = (wide * own_gain).astype(BF16)
        weights = wi[layer].reshape(P_SIZE, D // NT)
        partial = lax.dot_general(
            scaled, weights, (((1,), (1,)), ((), ())), preferred_element_type=F32
        ).astype(BF16)
        for j in range(NT):
            part[layer, h, j, 0:count] = partial[:, j * 128:(j + 1) * 128]
        for d in OTHERS:
            part_copy(h, layer, d, peer(d)).start()

    def pool(h, layer, tail):
        count = rows_in(h, layer)[1]
        start, out_count = rows_out(h, layer)
        seven = pl.ds(0, NT - 1)
        landed(ssq.at[layer, h, seven], sq_recv.at[layer, h])
        inv_rms = lax.rsqrt(jnp.sum(ssq[layer, h], axis=0) / D + EPS)
        inv_rms = jnp.broadcast_to(inv_rms, (128, 256)).T[0:count]
        total = part[layer, h, t, 0:count].astype(F32)
        landed(rs_in.at[layer, h, seven, pl.ds(0, count)], rs_recv.at[layer, h])
        for d in OTHERS:
            total = total + rs_in[layer, h, d, 0:count].astype(F32)
        pool_in = (total * inv_rms).astype(BF16).astype(F32)
        run = pool_in if tail is None else jnp.concatenate([tail, pool_in], axis=0)
        own = run[HALO:]
        picked = None
        for g in range(4):
            run = run + pltpu.roll(run, 1 << g, 0)
            picked = run if g == 0 else jnp.where(group >= g, run, picked)
        means = picked[HALO:] * inverse[start:start + out_count] - own
        own_scale = scale[pl.ds(layer, 1), pl.ds(lane1, 128)]
        mixed[layer, h, 0:out_count] = (means * own_scale).astype(BF16)
        for d in OTHERS:
            mixed_copy(h, layer, d, peer(d)).start()
        mix_in[layer, h, t, 0:out_count] = mixed[layer, h, 0:out_count]
        return pool_in[count - HALO:]

    def project_out(h, layer):
        start, count = rows_out(h, layer)
        landed(mix_in.at[layer, h, pl.ds(0, NT - 1), pl.ds(0, count)], mx_recv.at[layer, h])
        pooled = jnp.concatenate(
            [mix_in[layer, h, k, 0:count] for k in range(NT)], axis=1
        )
        branch = jnp.dot(
            pooled, wo[layer].reshape(P_SIZE, D // NT), preferred_element_type=F32
        )
        after = (state[start:start + count].astype(F32) + branch).astype(BF16)
        if layer == LAYERS - 1:
            out_ref[start - AHEAD:start - AHEAD + count] = after
        else:
            state[start:start + count] = after

    project_in(0, 0)
    advance("mid", 0)
    project_in(1, 0)
    for layer in range(LAYERS):
        advance("pool0", layer)
        tail = pool(0, layer, None)
        advance("pool1", layer)
        pool(1, layer, tail)
        advance("out0", layer)
        project_out(0, layer)
        if layer < LAYERS - 1:
            advance("in0", layer + 1)
            project_in(0, layer + 1)
        advance("out1", layer)
        project_out(1, layer)
        if layer < LAYERS - 1:
            project_in(1, layer + 1)

    def left(blocks, sem):
        remote(blocks, blocks, sem, sem, sp, t).wait_send()

    ahead.wait_send()
    for p in range(2 * LAYERS):
        if p in ROUND:
            left(piece(p).at[pl.ds(0, 15)], z_send.at[p])
            left(piece(p).at[pl.ds(0, 3), 0], y_send.at[p])
        else:
            left(piece(p).at[pl.ds(0, 15), 0], z_send.at[p])
            left(piece(p).at[pl.ds(0, 12)], y_send.at[p])
    seven = pl.ds(0, NT - 1)
    for layer in range(LAYERS):
        for h in (0, 1):
            count, out_count = rows_in(h, layer)[1], rows_out(h, layer)[1]
            left(ssq.at[layer, h, seven], sq_send.at[layer, h])
            left(part.at[layer, h, seven, pl.ds(0, count)], rs_send.at[layer, h])
            left(mix_in.at[layer, h, seven, pl.ds(0, out_count)], mx_send.at[layer, h])


def body(inputs, norm_gain, in_weight, pool_scale, out_weight):
    rows, features = inputs.shape
    vmem = pl.BlockSpec(memory_space=pltpu.VMEM)
    hbm = pl.BlockSpec(memory_space=pl.ANY)
    dma = pltpu.SemaphoreType.DMA
    pieces = 2 * LAYERS
    gathered = pltpu.VMEM((LAYERS, NZ, NY, P_SIZE // 64, features), BF16)
    most = AHEAD + SPLIT
    blocks = pltpu.VMEM((LAYERS, 2, NT, most, 128), BF16)
    return pl.pallas_call(
        kernel,
        out_shape=jax.ShapeDtypeStruct(inputs.shape, inputs.dtype),
        in_specs=[hbm] * 5,
        out_specs=vmem,
        scratch_shapes=[
            gathered, gathered,
            pltpu.VMEM((AHEAD + rows, features), BF16),
            pltpu.VMEM(norm_gain.shape, F32),
            pltpu.VMEM(pool_scale.shape, F32),
            pltpu.VMEM((AHEAD + rows, 128), F32),
            blocks, blocks,
            pltpu.VMEM((LAYERS, 2, NT, 1, rows), F32),
            pltpu.VMEM((LAYERS, 2, most, 128), BF16),
            blocks,
            dma((pieces,)), dma((pieces, 2)),
            dma((pieces,)), dma((pieces, 3)),
            dma((LAYERS, 2)), dma((LAYERS, 2)),
            dma((LAYERS, 2)), dma((LAYERS, 2)),
            dma((LAYERS, 2)), dma((LAYERS, 2)),
            dma((1,)), dma((1,)),
            dma((4,)), dma((2, 8)),
        ],
        compiler_params=pltpu.CompilerParams(
            collective_id=0, has_side_effects=True, vmem_limit_bytes=VMEM_LIMIT
        ),
        name="mixer",
    )(inputs, norm_gain, jnp.swapaxes(in_weight, 1, 2), pool_scale, out_weight)


def solution(mesh):
    placed = (P("sp", "tp"), P(), P(None, "tp", "sp"), P(), P(None, "sp", "tp"))
    return jax.shard_map(body, mesh=mesh, in_specs=placed, out_specs=P("sp", "tp"), check_vma=False)
```

time: 107 us -> 93.3 us (0.87)
  Pallas kernels: 105 us -> 91.5 us
    pallas_call x1, Pallas kernels: 105 us -> 91.5 us  [body(): pl.pallas_call(kernel, out_shape=jax.ShapeDtypeStruct(inputs.shape, input...]
where the time goes in v3:
time: 93.3 us; the launch traced here: 93.2 us
  Pallas kernels  91.5 us (98%)
  local copies, waits for them, and re-layouts  1.67 us (2%)
    pallas_call x1, Pallas kernels, body(): pl.pallas_call(kernel, out_shape=jax.ShapeDtypeStruct(inputs.shape, input...  91.5 us

profile of v3, /device:TPU:1, one launch (start us, length us, event | category | flops | bytes accessed | tf_op | source)
XLA Modules:
  0.0 93.2 jit_solution(337388349772858048)
XLA Ops:
  0.0 91.5 %mixer.1 = bf16[256,512]{1,0:T(8,128)(2,1)} custom-call(bf16[256,512]{1,0:T(8,128)(2,1)} %x_ref.1, f32[3,4096]{1,0:T(4,128)} %gain_ref.1, bf16[3,16,512]{2,1,0:T(8,128)(2,1)} %bitcast.1, f32[3,1024]{1,0:T(4,128)} %scale_ref.1, bf16[3,16,512]{2,1,0:T(8,128)(2,1)} %wout_ref.1), custom_call_target="tpu_custom_call" | custom-call | tf_op jit(solution)/shard_map/mixer/pallas_call | solution.py:326
  91.5 1.7 %copy.7 = bf16[256,512]{1,0:T(8,128)(2,1)} copy(bf16[256,512]{1,0:T(8,128)(2,1)} %mixer.1) | data formatting | bytes 524288

commit v4 on v3

--- a/solution.py
+++ b/solution.py
@@ -23,22 +23,47 @@
 RELAYS = ((-6, (2, 1, -1)), (6, (1, -1)), (-2, (2, 1, -1)), (2, (-2, -1, 1)))
 FIRST = (2, -6, -2, 6)
 LATER = (1, -1, 3, -3, 4, -4, 5, -5, 7, -7, 8)
-ROUND = (4, 5)
+ROUND = (5,)
 PLAN = {
     "start": (
-        (0, 0), (4, 0), (5, 0), (1, 0), (0, 1), (4, 1), (5, 1), (2, 0), (1, 1),
-        (0, 2), (4, 2), (3, 0), (0, 3), (2, 1), (1, 2), (5, 2), (4, 3), (0, 4),
-    ),
-    ("mid", 0): ((5, 3),),
-    ("pool0", 0): ((3, 1), (4, 4), (1, 3), (2, 2)),
-    ("pool1", 0): ((4, 5), (5, 4)),
-    ("out0", 0): ((1, 4), (4, 6), (5, 5), (2, 3), (3, 2)),
-    ("in0", 1): ((2, 4),),
-    ("out1", 0): ((4, 7), (5, 6)),
-    ("pool0", 1): ((3, 3), (4, 8), (5, 7)),
-    ("pool1", 1): ((4, 9), (5, 8)),
-    ("out0", 1): ((3, 4), (4, 10), (5, 9)),
-    ("out1", 1): ((5, 10),),
+        (0, 0), (5, 0), (1, 0), (0, 1), (5, 1), (2, 0), (1, 1), (0, 2), (5, 2), (3, 0), (0, 3), (2, 1), (1, 2), (5, 3), (0, 4),
+    ),
+    ("pre0", 0): (
+        (2, 2), (3, 1), (4, 0),
+    ),
+    ("pool0", 0): (
+        (1, 3), (5, 4),
+    ),
+    ("pool1", 0): (
+        (5, 5), (4, 1),
+    ),
+    ("out0", 0): (
+        (1, 4), (2, 3), (3, 2), (5, 6),
+    ),
+    ("in0", 1): (
+        (2, 4),
+    ),
+    ("pre0", 1): (
+        (4, 2),
+    ),
+    ("out1", 0): (
+        (5, 7),
+    ),
+    ("pool0", 1): (
+        (3, 3), (5, 8),
+    ),
+    ("pool1", 1): (
+        (4, 3),
+    ),
+    ("out0", 1): (
+        (3, 4), (5, 9),
+    ),
+    ("in0", 2): (
+        (4, 4),
+    ),
+    ("out1", 1): (
+        (5, 10),
+    ),
 }
 
 
@@ -51,9 +76,9 @@
 
 def kernel(
     x_ref, gain_ref, win_ref, scale_ref, wout_ref, out_ref,
-    wi, wo, state, gain, scale, inverse, part, rs_in, ssq, mixed, mix_in,
+    wi, wo, state, gain, scale, inverse, part, pair, both, rs_in, ssq, mixed, mix_in,
     z_send, z_recv, y_send, y_recv, rs_send, rs_recv,
-    sq_send, sq_recv, mx_send, mx_recv, h_send, h_recv, own_sem, r_recv,
+    sq_send, sq_recv, mx_send, mx_recv, pair_send, pair_recv, px_recv, h_send, h_recv, own_sem, r_recv,
 ):
     sp = lax.axis_index("sp")
     t = lax.axis_index("tp")
@@ -124,20 +149,24 @@
         if k == 2:
             landed(piece(p).at[pl.ds(0, 11), 0], z_recv.at[p, 1])
             for way in (1, -1):
-                for offset in LATER:
+                for offset in LATER[:5] if way > 0 else LATER[5:]:
                     along_y(p, offset, 0, way, 1)
+            for way in (1, -1):
+                for offset in LATER[5:] if way > 0 else LATER[:5]:
+                    along_y(p, offset, 0, way, 3)
             landed(piece(p).at[pl.ds(0, 5), pl.ds(0, 2)], y_recv.at[p, 0])
             for offset in (0, 2, -6):
                 along_y(p, offset, -1, 1, 2)
             for offset in (-2, 6):
                 along_y(p, offset, 1, -1, 2)
         if k == 3:
-            landed(piece(p).at[pl.ds(0, 11), pl.ds(0, 2)], y_recv.at[p, 1])
+            landed(piece(p).at[pl.ds(0, 11), 0], y_recv.at[p, 1])
             for offset in LATER[:5]:
                 along_y(p, offset, -1, 1, 2)
             for offset in LATER[5:]:
                 along_y(p, offset, 1, -1, 2)
         if k == 4:
+            landed(piece(p).at[pl.ds(0, 11), 0], y_recv.at[p, 3])
             landed(piece(p).at[:, 0], y_recv.at[p, 2])
 
     def ring_copy(p, way, step):
@@ -195,11 +224,24 @@
         start, count = rows_in(h, layer)
         return (start, count) if h else (start + HALO, count - HALO)
 
-    def part_copy(h, layer, d, j):
+    chip, core = t // 2, t % 2
+    partner = chip * 2 + 1 - core
+
+    def same_core(dx):
+        return ((chip + dx) % 4) * 2 + core
+
+    def pair_copy(h, layer):
         rows = pl.ds(0, rows_in(h, layer)[1])
         return remote(
-            part.at[layer, h, j, rows], rs_in.at[layer, h, d, rows],
-            rs_send.at[layer, h], rs_recv.at[layer, h], sp, j,
+            part.at[layer, h, 1 - core, :, rows], pair.at[layer, h, :, rows],
+            pair_send.at[layer, h], pair_recv.at[layer, h], sp, partner,
+        )
+
+    def sum_copy(h, layer, dx):
+        rows = pl.ds(0, rows_in(h, layer)[1])
+        return remote(
+            both.at[layer, h, dx, rows], rs_in.at[layer, h, dx, rows],
+            rs_send.at[layer, h], rs_recv.at[layer, h], sp, same_core(dx),
         )
 
     def square_copy(h, layer, d, j):
@@ -208,11 +250,11 @@
             sq_send.at[layer, h], sq_recv.at[layer, h], sp, j,
         )
 
-    def mixed_copy(h, layer, d, j):
+    def mixed_copy(h, layer, j, recv):
         rows = pl.ds(0, rows_out(h, layer)[1])
         return remote(
             mixed.at[layer, h, rows], mix_in.at[layer, h, t, rows],
-            mx_send.at[layer, h], mx_recv.at[layer, h], sp, j,
+            mx_send.at[layer, h], recv.at[layer, h], sp, j,
         )
 
     def project_in(h, layer):
@@ -231,9 +273,21 @@
             scaled, weights, (((1,), (1,)), ((), ())), preferred_element_type=F32
         ).astype(BF16)
         for j in range(NT):
-            part[layer, h, j, 0:count] = partial[:, j * 128:(j + 1) * 128]
-        for d in OTHERS:
-            part_copy(h, layer, d, peer(d)).start()
+            part[layer, h, j % 2, j // 2, 0:count] = partial[:, j * 128:(j + 1) * 128]
+        pair_copy(h, layer).start()
+
+    def chip_sum(h, layer, to):
+        count = rows_in(h, layer)[1]
+        own = part[layer, h, core, to, 0:count].astype(F32)
+        return own + pair[layer, h, to, 0:count].astype(F32)
+
+    def combine(h, layer):
+        count = rows_in(h, layer)[1]
+        landed(pair.at[layer, h, :, pl.ds(0, count)], pair_recv.at[layer, h])
+        for dx in (2, 1, 3):
+            total = chip_sum(h, layer, (chip + dx) % 4)
+            both[layer, h, dx, 0:count] = total.astype(BF16)
+            sum_copy(h, layer, dx).start()
 
     def pool(h, layer, tail):
         count = rows_in(h, layer)[1]
@@ -242,10 +296,10 @@
         landed(ssq.at[layer, h, seven], sq_recv.at[layer, h])
         inv_rms = lax.rsqrt(jnp.sum(ssq[layer, h], axis=0) / D + EPS)
         inv_rms = jnp.broadcast_to(inv_rms, (128, 256)).T[0:count]
-        total = part[layer, h, t, 0:count].astype(F32)
-        landed(rs_in.at[layer, h, seven, pl.ds(0, count)], rs_recv.at[layer, h])
-        for d in OTHERS:
-            total = total + rs_in[layer, h, d, 0:count].astype(F32)
+        total = chip_sum(h, layer, chip)
+        landed(rs_in.at[layer, h, pl.ds(0, 3), pl.ds(0, count)], rs_recv.at[layer, h])
+        for dx in (1, 2, 3):
+            total = total + rs_in[layer, h, dx, 0:count].astype(F32)
         pool_in = (total * inv_rms).astype(BF16).astype(F32)
         run = pool_in if tail is None else jnp.concatenate([tail, pool_in], axis=0)
         own = run[HALO:]
@@ -256,14 +310,24 @@
         means = picked[HALO:] * inverse[start:start + out_count] - own
         own_scale = scale[pl.ds(layer, 1), pl.ds(lane1, 128)]
         mixed[layer, h, 0:out_count] = (means * own_scale).astype(BF16)
-        for d in OTHERS:
-            mixed_copy(h, layer, d, peer(d)).start()
+        for dx in (2, 1, 3):
+            mixed_copy(h, layer, same_core(dx), mx_recv).start()
+        mixed_copy(h, layer, partner, px_recv).start()
         mix_in[layer, h, t, 0:out_count] = mixed[layer, h, 0:out_count]
         return pool_in[count - HALO:]
 
+    def relay(h, layer):
+        rows = pl.ds(0, rows_out(h, layer)[1])
+        landed(mix_in.at[layer, h, pl.ds(0, 3), rows], mx_recv.at[layer, h])
+        for dx in (1, 2, 3):
+            block = mix_in.at[layer, h, same_core(dx), rows]
+            remote(
+                block, block, mx_send.at[layer, h], px_recv.at[layer, h], sp, partner
+            ).start()
+
     def project_out(h, layer):
         start, count = rows_out(h, layer)
-        landed(mix_in.at[layer, h, pl.ds(0, NT - 1), pl.ds(0, count)], mx_recv.at[layer, h])
+        landed(mix_in.at[layer, h, pl.ds(0, 4), pl.ds(0, count)], px_recv.at[layer, h])
         pooled = jnp.concatenate(
             [mix_in[layer, h, k, 0:count] for k in range(NT)], axis=1
         )
@@ -277,22 +341,29 @@
             state[start:start + count] = after
 
     project_in(0, 0)
-    advance("mid", 0)
+    advance("pre0", 0)
+    combine(0, 0)
     project_in(1, 0)
+    combine(1, 0)
     for layer in range(LAYERS):
         advance("pool0", layer)
         tail = pool(0, layer, None)
         advance("pool1", layer)
         pool(1, layer, tail)
         advance("out0", layer)
+        relay(0, layer)
         project_out(0, layer)
         if layer < LAYERS - 1:
             advance("in0", layer + 1)
             project_in(0, layer + 1)
+            advance("pre0", layer + 1)
+            combine(0, layer + 1)
         advance("out1", layer)
+        relay(1, layer)
         project_out(1, layer)
         if layer < LAYERS - 1:
             project_in(1, layer + 1)
+            combine(1, layer + 1)
 
     def left(blocks, sem):
         remote(blocks, blocks, sem, sem, sp, t).wait_send()
@@ -310,7 +381,8 @@
         for h in (0, 1):
             count, out_count = rows_in(h, layer)[1], rows_out(h, layer)[1]
             left(ssq.at[layer, h, seven], sq_send.at[layer, h])
-            left(part.at[layer, h, seven, pl.ds(0, count)], rs_send.at[layer, h])
+            left(pair.at[layer, h, :, pl.ds(0, count)], pair_send.at[layer, h])
+            left(both.at[layer, h, pl.ds(0, 3), pl.ds(0, count)], rs_send.at[layer, h])
             left(mix_in.at[layer, h, seven, pl.ds(0, out_count)], mx_send.at[layer, h])
 
 
@@ -323,6 +395,7 @@
     gathered = pltpu.VMEM((LAYERS, NZ, NY, P_SIZE // 64, features), BF16)
     most = AHEAD + SPLIT
     blocks = pltpu.VMEM((LAYERS, 2, NT, most, 128), BF16)
+    quarter = pltpu.VMEM((LAYERS, 2, 4, most, 128), BF16)
     return pl.pallas_call(
         kernel,
         out_shape=jax.ShapeDtypeStruct(inputs.shape, inputs.dtype),
@@ -334,15 +407,17 @@
             pltpu.VMEM(norm_gain.shape, F32),
             pltpu.VMEM(pool_scale.shape, F32),
             pltpu.VMEM((AHEAD + rows, 128), F32),
-            blocks, blocks,
+            pltpu.VMEM((LAYERS, 2, 2, 4, most, 128), BF16),
+            quarter, quarter, quarter,
             pltpu.VMEM((LAYERS, 2, NT, 1, rows), F32),
             pltpu.VMEM((LAYERS, 2, most, 128), BF16),
             blocks,
             dma((pieces,)), dma((pieces, 2)),
-            dma((pieces,)), dma((pieces, 3)),
+            dma((pieces,)), dma((pieces, 4)),
             dma((LAYERS, 2)), dma((LAYERS, 2)),
             dma((LAYERS, 2)), dma((LAYERS, 2)),
             dma((LAYERS, 2)), dma((LAYERS, 2)),
+            dma((LAYERS, 2)), dma((LAYERS, 2)), dma((LAYERS, 2)),
             dma((1,)), dma((1,)),
             dma((4,)), dma((2, 8)),
         ],

time: 93.3 us -> 88.3 us (0.946)
  Pallas kernels: 91.5 us -> 86.4 us
    pallas_call x1, Pallas kernels: 91.5 us -> 86.4 us  [body(): pl.pallas_call(kernel, out_shape=jax.ShapeDtypeStruct(inputs.shape, input...]
where the time goes in v4:
time: 88.3 us; the launch traced here: 88.1 us
  Pallas kernels  86.4 us (98%)
  local copies, waits for them, and re-layouts  1.67 us (2%)
    pallas_call x1, Pallas kernels, body(): pl.pallas_call(kernel, out_shape=jax.ShapeDtypeStruct(inputs.shape, input...  86.4 us

profile of v4, /device:TPU:1, one launch (start us, length us, event | category | flops | bytes accessed | tf_op | source)
XLA Modules:
  0.0 88.1 jit_solution(2726507937520035918)
XLA Ops:
  0.0 86.4 %mixer.1 = bf16[256,512]{1,0:T(8,128)(2,1)} custom-call(bf16[256,512]{1,0:T(8,128)(2,1)} %x_ref.1, f32[3,4096]{1,0:T(4,128)} %gain_ref.1, bf16[3,16,512]{2,1,0:T(8,128)(2,1)} %bitcast.1, f32[3,1024]{1,0:T(4,128)} %scale_ref.1, bf16[3,16,512]{2,1,0:T(8,128)(2,1)} %wout_ref.1), custom_call_target="tpu_custom_call" | custom-call | tf_op jit(solution)/shard_map/mixer/pallas_call | solution.py:399
  86.4 1.7 %copy.7 = bf16[256,512]{1,0:T(8,128)(2,1)} copy(bf16[256,512]{1,0:T(8,128)(2,1)} %mixer.1) | data formatting | bytes 524288

commit v5 on v4

--- a/solution.py
+++ b/solution.py
@@ -12,7 +12,7 @@
 LAYERS = 3
 EPS = 1e-06
 HALO = 16
-AHEAD, SPLIT = 48, 112
+AHEAD, SPLIT = 48, 128
 NZ, NY, NT = 16, 4, 8
 MESH = pl.DeviceIdType.MESH
 BF16, F32 = jnp.bfloat16, jnp.float32
@@ -26,10 +26,10 @@
 ROUND = (5,)
 PLAN = {
     "start": (
-        (0, 0), (5, 0), (1, 0), (0, 1), (5, 1), (2, 0), (1, 1), (0, 2), (5, 2), (3, 0), (0, 3), (2, 1), (1, 2), (5, 3), (0, 4),
+        (0, 0), (5, 0), (1, 0), (0, 1), (5, 1), (2, 0), (1, 1), (0, 2), (5, 2), (3, 0), (0, 3), (2, 1), (1, 2), (4, 0), (5, 3), (0, 4),
     ),
     ("pre0", 0): (
-        (2, 2), (3, 1), (4, 0),
+        (2, 2), (3, 1),
     ),
     ("pool0", 0): (
         (1, 3), (5, 4),
@@ -260,12 +260,6 @@
     def project_in(h, layer):
         start, count = rows_in(h, layer)
         wide = state[start:start + count].astype(F32)
-        squares = jnp.sum(wide * wide, axis=1, keepdims=True)
-        squares = jnp.broadcast_to(squares, (count, 128))
-        squares = jnp.concatenate([squares, jnp.zeros((256 - count, 128), F32)], axis=0)
-        ssq[layer, h, t] = squares.T[0:1, :]
-        for d in OTHERS:
-            square_copy(h, layer, d, peer(d)).start()
         own_gain = gain[pl.ds(layer, 1), pl.ds(lane0, D // NT)]
         scaled = (wide * own_gain).astype(BF16)
         weights = wi[layer].reshape(P_SIZE, D // NT)
@@ -275,6 +269,12 @@
         for j in range(NT):
             part[layer, h, j % 2, j // 2, 0:count] = partial[:, j * 128:(j + 1) * 128]
         pair_copy(h, layer).start()
+        squares = jnp.sum(wide * wide, axis=1, keepdims=True)
+        squares = jnp.broadcast_to(squares, (count, 128))
+        squares = jnp.concatenate([squares, jnp.zeros((256 - count, 128), F32)], axis=0)
+        ssq[layer, h, t] = squares.T[0:1, :]
+        for d in OTHERS:
+            square_copy(h, layer, d, peer(d)).start()
 
     def chip_sum(h, layer, to):
         count = rows_in(h, layer)[1]

time: 88.3 us -> 87 us (0.985)
  Pallas kernels: 86.4 us -> 85.2 us
    pallas_call x1, Pallas kernels: 86.4 us -> 85.2 us  [body(): pl.pallas_call(kernel, out_shape=jax.ShapeDtypeStruct(inputs.shape, input...]
where the time goes in v5:
time: 87 us; the launch traced here: 86.8 us
  Pallas kernels  85.2 us (98%)
  local copies, waits for them, and re-layouts  1.67 us (2%)
    pallas_call x1, Pallas kernels, body(): pl.pallas_call(kernel, out_shape=jax.ShapeDtypeStruct(inputs.shape, input...  85.2 us

profile of v5, /device:TPU:1, one launch (start us, length us, event | category | flops | bytes accessed | tf_op | source)
XLA Modules:
  0.0 86.8 jit_solution(10400777742499258346)
XLA Ops:
  0.0 85.2 %mixer.1 = bf16[256,512]{1,0:T(8,128)(2,1)} custom-call(bf16[256,512]{1,0:T(8,128)(2,1)} %x_ref.1, f32[3,4096]{1,0:T(4,128)} %gain_ref.1, bf16[3,16,512]{2,1,0:T(8,128)(2,1)} %bitcast.1, f32[3,1024]{1,0:T(4,128)} %scale_ref.1, bf16[3,16,512]{2,1,0:T(8,128)(2,1)} %wout_ref.1), custom_call_target="tpu_custom_call" | custom-call | tf_op jit(solution)/shard_map/mixer/pallas_call | solution.py:399
  85.2 1.7 %copy.7 = bf16[256,512]{1,0:T(8,128)(2,1)} copy(bf16[256,512]{1,0:T(8,128)(2,1)} %mixer.1) | data formatting | bytes 524288

commit v6 on v5

--- a/solution.py
+++ b/solution.py
@@ -29,16 +29,16 @@
         (0, 0), (5, 0), (1, 0), (0, 1), (5, 1), (2, 0), (1, 1), (0, 2), (5, 2), (3, 0), (0, 3), (2, 1), (1, 2), (4, 0), (5, 3), (0, 4),
     ),
     ("pre0", 0): (
-        (2, 2), (3, 1),
+        (1, 3, 1), (2, 2), (3, 1),
     ),
     ("pool0", 0): (
-        (1, 3), (5, 4),
+        (1, 3, 0), (5, 4),
     ),
     ("pool1", 0): (
         (5, 5), (4, 1),
     ),
     ("out0", 0): (
-        (1, 4), (2, 3), (3, 2), (5, 6),
+        (1, 4), (3, 2), (5, 6),
     ),
     ("in0", 1): (
         (2, 4),
@@ -63,6 +63,9 @@
     ),
     ("out1", 1): (
         (5, 10),
+    ),
+    ("pass0", 0): (
+        (2, 3),
     ),
 }
 
@@ -193,11 +196,12 @@
                 ring_copy(p, way, k - 2)
 
     def advance(*where):
-        for p, k in PLAN.get(where[0] if len(where) == 1 else where, ()):
-            if p in ROUND:
-                ring_stage(p, k)
+        for p, k, *only in PLAN.get(where[0] if len(where) == 1 else where, ()):
+            run = functools.partial(ring_stage if p in ROUND else stage, p, k)
+            if only:
+                pl.when(t % 2 == only[0])(run)
             else:
-                stage(p, k)
+                run()
 
     ahead = remote(
         x_ref.at[pl.ds(256 - AHEAD, AHEAD)], state.at[pl.ds(0, AHEAD)],
@@ -350,16 +354,17 @@
         tail = pool(0, layer, None)
         advance("pool1", layer)
         pool(1, layer, tail)
+        advance("pass0", layer)
+        relay(0, layer)
         advance("out0", layer)
-        relay(0, layer)
         project_out(0, layer)
         if layer < LAYERS - 1:
             advance("in0", layer + 1)
             project_in(0, layer + 1)
             advance("pre0", layer + 1)
             combine(0, layer + 1)
+        relay(1, layer)
         advance("out1", layer)
-        relay(1, layer)
         project_out(1, layer)
         if layer < LAYERS - 1:
             project_in(1, layer + 1)

time: 87 us -> 85.9 us (0.987)
  Pallas kernels: 85.2 us -> 84.1 us
    pallas_call x1, Pallas kernels: 85.2 us -> 84.1 us  [body(): pl.pallas_call(kernel, out_shape=jax.ShapeDtypeStruct(inputs.shape, input...]
where the time goes in v6:
time: 85.9 us; the launch traced here: 85.7 us
  Pallas kernels  84.1 us (98%)
  local copies, waits for them, and re-layouts  1.67 us (2%)
    pallas_call x1, Pallas kernels, body(): pl.pallas_call(kernel, out_shape=jax.ShapeDtypeStruct(inputs.shape, input...  84.1 us

profile of v6, /device:TPU:1, one launch (start us, length us, event | category | flops | bytes accessed | tf_op | source)
XLA Modules:
  0.0 85.7 jit_solution(12934193104725662720)
XLA Ops:
  0.0 84.1 %mixer.1 = bf16[256,512]{1,0:T(8,128)(2,1)} custom-call(bf16[256,512]{1,0:T(8,128)(2,1)} %x_ref.1, f32[3,4096]{1,0:T(4,128)} %gain_ref.1, bf16[3,16,512]{2,1,0:T(8,128)(2,1)} %bitcast.1, f32[3,1024]{1,0:T(4,128)} %scale_ref.1, bf16[3,16,512]{2,1,0:T(8,128)(2,1)} %wout_ref.1), custom_call_target="tpu_custom_call" | custom-call | tf_op jit(solution)/shard_map/mixer/pallas_call | solution.py:404
  84.1 1.7 %copy.7 = bf16[256,512]{1,0:T(8,128)(2,1)} copy(bf16[256,512]{1,0:T(8,128)(2,1)} %mixer.1) | data formatting | bytes 524288

commit v7 on v6

--- a/solution.py
+++ b/solution.py
@@ -362,8 +362,9 @@
             advance("in0", layer + 1)
             project_in(0, layer + 1)
             advance("pre0", layer + 1)
+        relay(1, layer)
+        if layer < LAYERS - 1:
             combine(0, layer + 1)
-        relay(1, layer)
         advance("out1", layer)
         project_out(1, layer)
         if layer < LAYERS - 1:

time: 85.9 us -> 85.6 us (level)
  no operation moved by 1% of the time
where the time goes in v7:
time: 85.6 us; the launch traced here: 85.4 us
  Pallas kernels  83.7 us (98%)
  local copies, waits for them, and re-layouts  1.67 us (2%)
    pallas_call x1, Pallas kernels, body(): pl.pallas_call(kernel, out_shape=jax.ShapeDtypeStruct(inputs.shape, input...  83.7 us

profile of v7, /device:TPU:1, one launch (start us, length us, event | category | flops | bytes accessed | tf_op | source)
XLA Modules:
  0.0 85.4 jit_solution(13080431975484909850)
XLA Ops:
  0.0 83.7 %mixer.1 = bf16[256,512]{1,0:T(8,128)(2,1)} custom-call(bf16[256,512]{1,0:T(8,128)(2,1)} %x_ref.1, f32[3,4096]{1,0:T(4,128)} %gain_ref.1, bf16[3,16,512]{2,1,0:T(8,128)(2,1)} %bitcast.1, f32[3,1024]{1,0:T(4,128)} %scale_ref.1, bf16[3,16,512]{2,1,0:T(8,128)(2,1)} %wout_ref.1), custom_call_target="tpu_custom_call" | custom-call | tf_op jit(solution)/shard_map/mixer/pallas_call | solution.py:405
  83.7 1.7 %copy.7 = bf16[256,512]{1,0:T(8,128)(2,1)} copy(bf16[256,512]{1,0:T(8,128)(2,1)} %mixer.1) | data formatting | bytes 524288
